TPU v7x, 32 devices: a whole 2x2x4 slice. The times are simulated.
32 devices in a mesh: grp: 2 (over y), fs: 4 (over z), tp: 4 (over x, core).
Axes of the slice: x: 2, y: 2, z: 4, core: 2. Of those that a mesh axis runs over, the one named last changes fastest.
Arguments:
- prompt: bfloat16 [8, 1024, 2048], P(('grp', 'tp')), parts along dimension 0, may hold values from -6 to 6
- gate_first: float32 [2048, 5632], P('fs', 'tp'), may hold values from -0.125 to 0.125
- up_first: float32 [2048, 5632], P('fs', 'tp'), may hold values from -0.125 to 0.125
- down_first: float32 [5632, 2048], P('fs', 'tp'), may hold values from -0.3125 to 0.3125
- norm_gain: float32 [2048], replicated, may hold values from 0.1 to 1.9
- gate_second: float32 [2048, 5632], P('fs', 'tp'), may hold values from -0.125 to 0.125
- up_second: float32 [2048, 5632], P('fs', 'tp'), may hold values from -0.125 to 0.125
- down_second: float32 [5632, 2048], P('fs', 'tp'), may hold values from -0.3125 to 0.3125
Outputs:
- result: bfloat16 [8, 1024, 2048], P(('grp', 'tp'), 'fs'), parts along dimension 0
- gate_one: bfloat16 [4096, 5632], P('grp', 'fs'), parts along dimension 0
- up_one: bfloat16 [4096, 5632], P('grp', 'fs'), parts along dimension 0
- down_one: bfloat16 [5632, 4096], P('fs', 'grp'), parts along dimension 1
- gate_two: bfloat16 [4096, 5632], P('grp', 'fs'), parts along dimension 0
- up_two: bfloat16 [4096, 5632], P('grp', 'fs'), parts along dimension 0
- down_two: bfloat16 [5632, 4096], P('fs', 'grp'), parts along dimension 1
There are 2 independent parts, one for each index of `grp`. A program takes and returns all parts, laid end to end along the dimension named above; an argument that names none is the same for every part. Nothing has to cross between parts.
All inputs are finite; a program needn't handle non-finite values.
Results may differ from a plain program's by a relative error of at most 0.029.
Values may be sent and summed in bfloat16 or wider, within the bound.
No kernel may reach another device: no remote copies, remote signals or barrier semaphores. Data moves between devices by JAX's collectives and lax.ppermute only.
A program may use at most 192 MiB of HBM per device.

v0:
```python
import jax
import jax.numpy as jnp
from jax import lax
from jax.sharding import PartitionSpec as P

norm_eps = 1e-05
deep_alpha = 2.0**0.25
half_step = 0.5


def plain_norm(values):
    row_mean = jnp.mean(values, axis=-1, keepdims=True)
    centred = values - row_mean
    variance = jnp.mean(centred * centred, axis=-1, keepdims=True)
    return centred * lax.rsqrt(variance + norm_eps)


def gated_hidden(inputs, gate_proj, up_proj):
    gate_act = jnp.dot(inputs, gate_proj, preferred_element_type=jnp.float32)
    up_act = jnp.dot(inputs, up_proj, preferred_element_type=jnp.float32)
    return (jax.nn.silu(gate_act) * up_act).astype(jnp.bfloat16)


def relay_weights(gate_proj, up_proj, down_proj):
    gate_rows, up_rows, down_mine = (
        lax.all_gather(gate_proj, "tp", axis=1, tiled=True),
        lax.all_gather(up_proj, "tp", axis=1, tiled=True),
        lax.all_gather(down_proj, "tp", axis=1, tiled=True),
    )
    gate_mine, up_mine = (
        lax.all_to_all(gate_rows, "fs", split_axis=1, concat_axis=0, tiled=True),
        lax.all_to_all(up_rows, "fs", split_axis=1, concat_axis=0, tiled=True),
    )
    return (gate_mine, up_mine, down_mine)


def row_terms(hidden, down_proj):
    return jnp.dot(hidden, down_proj, preferred_element_type=jnp.float32)


def body(prompt, gate_first, up_first, down_first, norm_gain, gate_second, up_second, down_second):
    fs_index = lax.axis_index("fs")
    row_block = gate_first.shape[0]
    gain_rows = lax.dynamic_slice_in_dim(norm_gain, fs_index * row_block, row_block, 0)
    gate_one, up_one, down_one = relay_weights(
        gate_first.astype(jnp.bfloat16),
        up_first.astype(jnp.bfloat16),
        down_first.astype(jnp.bfloat16),
    )
    gate_two, up_two, down_two = relay_weights(
        (gain_rows[:, None] * gate_second).astype(jnp.bfloat16),
        (gain_rows[:, None] * up_second).astype(jnp.bfloat16),
        down_second.astype(jnp.bfloat16),
    )
    tokens = prompt.reshape(-1, prompt.shape[-1])
    own_count = tokens.shape[0] // lax.axis_size("fs")
    own_first = fs_index * own_count
    hidden_one = gated_hidden(tokens, gate_one, up_one)
    own_tokens = lax.dynamic_slice_in_dim(tokens, own_first, own_count, 0)
    ffn_one = lax.psum_scatter(
        row_terms(hidden_one, down_one).astype(jnp.bfloat16), "fs", scatter_dimension=0, tiled=True
    ).astype(jnp.float32)
    normed_own = plain_norm(
        deep_alpha * own_tokens.astype(jnp.float32) + half_step * ffn_one
    ).astype(jnp.bfloat16)
    hidden_two = gated_hidden(
        lax.all_gather(normed_own, "fs", axis=0, tiled=True), gate_two, up_two
    )
    ffn_two = lax.psum_scatter(
        row_terms(hidden_two, down_two).astype(jnp.bfloat16), "fs", scatter_dimension=0, tiled=True
    ).astype(jnp.float32)
    residual_two = deep_alpha * norm_gain * normed_own.astype(jnp.float32)
    result = plain_norm(residual_two + half_step * ffn_two).astype(jnp.bfloat16)
    return (
        result.reshape(1, result.shape[0], result.shape[-1]),
        gate_one,
        up_one,
        down_one,
        gate_two,
        up_two,
        down_two,
    )


def solution(mesh):
    placed = (
        P(("grp", "tp"), None, None),
        P("fs", "tp"),
        P("fs", "tp"),
        P("fs", "tp"),
        P(),
        P("fs", "tp"),
        P("fs", "tp"),
        P("fs", "tp"),
    )
    return jax.shard_map(
        body,
        mesh=mesh,
        in_specs=placed,
        out_specs=(
            P(("grp", "tp"), "fs", None),
            P("grp", "fs"),
            P("grp", "fs"),
            P("fs", "grp"),
            P("grp", "fs"),
            P("grp", "fs"),
            P("fs", "grp"),
        ),
        check_vma=False,
    )
```

profile of v0, /device:TPU:0, one launch (start us, length us, event | category | flops | bytes accessed | tf_op | source)
XLA Modules:
  0.0 934.5 jit_solution(12915030123418314235)
XLA Ops:
  11.8 44.9 %all-gather.8.cloned.1.call-done = bf16[512,5632]{1,0:T(8,128)(2,1)} async-done(((bf16[512,1408]{1,0:T(8,128)(2,1)}), bf16[512,5632]{1,0:T(8,128)(2,1)}) %all-gather.8.cloned.1.call-update) | async-done | bytes 5767184 | tf_op jit(solution)/shard_map/all_gather | solution.py:26
  56.7 5.6 copy.30
  62.3 5.5 all-to-all-start
  69.2 33.0 %all-gather.10.cloned.1.call-done = bf16[512,5632]{1,0:T(8,128)(2,1)} async-done(((bf16[512,1408]{1,0:T(8,128)(2,1)}), bf16[512,5632]{1,0:T(8,128)(2,1)}) %all-gather.10.cloned.1.call-update) | async-done | bytes 5767184 | tf_op jit(solution)/shard_map/all_gather | solution.py:27
  102.2 5.6 copy.29
  107.8 87.6 %all-to-all-done = bf16[512,4,1408]{2,0,1:T(8,128)(2,1)} async-done(((bf16[512,4,1408]{2,0,1:T(8,128)(2,1)}), bf16[512,4,1408]{2,0,1:T(8,128)(2,1)}, u32[]{:S(2)}, u32[]{:S(2)}) %all-to-all-start) | async-done | bytes 5767200 | tf_op jit(solution)/shard_map/all_to_all | solution.py:31
  195.4 5.5 all-to-all-start.1
  205.1 11.7 %fusion.1 = f32[1024,1408]{1,0:T(8,128)} fusion(bf16[2048,1408]{1,0:T(8,128)(2,1)} %bitcast.3, bf16[1,1024,2048]{2,1,0:T(8,128)(2,1)} %param.8), kind=kOutput, calls=%fused_computation.7 | convolution fusion | flops 5905580032 | bytes 15728640 | tf_op jit(solution)/shard_map/dot_general | solution.py:19
  216.8 110.9 %all-to-all-done.1 = bf16[512,4,1408]{2,0,1:T(8,128)(2,1)} async-done(((bf16[512,4,1408]{2,0,1:T(8,128)(2,1)}), bf16[512,4,1408]{2,0,1:T(8,128)(2,1)}, u32[]{:S(2)}, u32[]{:S(2)}) %all-to-all-start.1) | async-done | bytes 5767200 | tf_op jit(solution)/shard_map/all_to_all | solution.py:32
  327.7 20.6 %convolution_convert_fusion.1 = bf16[1024,2048]{1,0:T(8,128)(2,1)} fusion(bf16[1408,2048]{1,0:T(8,128)(2,1)} %all-gather.12.cloned.1.call-done, f32[1024,1408]{1,0:T(8,128)} %fusion.1, bf16[2048,1408]{1,0:T(8,128)(2,1)} %bitcast.5, bf16[1,1024,2048]{2,1,0:T(8,128)(2,1)} %param.8), kind=kOutput, calls=%fused_computation.10 | convolution fusion | flops 11821907968 | bytes 25690112 | tf_op jit(solution)/shard_map/dot_general | solution.py:38
  348.9 5.6 copy.28
  359.7 124.0 %reduce-scatter.3.cloned.1.call-done = bf16[256,2048]{1,0:T(8,128)(2,1)} async-done(((bf16[1024,2048]{1,0:T(8,128)(2,1)}), bf16[256,2048]{1,0:T(8,128)(2,1)}) %reduce-scatter.3.cloned.1.call-update) | async-done | bytes 1048592 | tf_op jit(solution)/shard_map/reduce_scatter | solution.py:60
  492.3 82.7 %all-gather.18.cloned.1.call-done = bf16[512,5632]{1,0:T(8,128)(2,1)} async-done(((bf16[512,1408]{1,0:T(8,128)(2,1)}), bf16[512,5632]{1,0:T(8,128)(2,1)}) %all-gather.18.cloned.1.call-update) | async-done | bytes 5767184 | tf_op jit(solution)/shard_map/all_gather | solution.py:27
  575.0 5.6 copy.27
  580.6 5.3 all-to-all-start.3
  585.9 167.0 %all-gather.14.cloned.1.call-done = bf16[1024,2048]{1,0:T(8,128)(2,1)} async-done(((bf16[256,2048]{1,0:T(8,128)(2,1)}), bf16[1024,2048]{1,0:T(8,128)(2,1)}) %all-gather.14.cloned.1.call-update) | async-done | bytes 4194320 | tf_op jit(solution)/shard_map/all_gather | solution.py:67
  753.0 11.7 %fusion.6 = f32[1024,1408]{1,0:T(8,128)} fusion(bf16[1024,2048]{1,0:T(8,128)(2,1)} %all-gather.14.cloned.1.call-done, bf16[2048,1408]{1,0:T(8,128)(2,1)} %bitcast.7), kind=kOutput, calls=%fused_computation.27 | convolution fusion | flops 5905580032 | bytes 15728640 | tf_op jit(solution)/shard_map/dot_general | solution.py:19
  764.7 32.5 %all-gather.20.cloned.1.call-done = bf16[1408,2048]{1,0:T(8,128)(2,1)} async-done(((bf16[1408,512]{1,0:T(8,128)(2,1)}), bf16[1408,2048]{1,0:T(8,128)(2,1)}) %all-gather.20.cloned.1.call-update) | async-done | bytes 5767184 | tf_op jit(solution)/shard_map/all_gather | solution.py:28
  797.2 20.6 %convolution_convert_fusion = bf16[1024,2048]{1,0:T(8,128)(2,1)} fusion(bf16[1408,2048]{1,0:T(8,128)(2,1)} %all-gather.20.cloned.1.call-done, f32[1024,1408]{1,0:T(8,128)} %fusion.6, bf16[1024,2048]{1,0:T(8,128)(2,1)} %all-gather.14.cloned.1.call-done, bf16[2048,1408]{1,0:T(8,128)(2,1)} %bitcast.9), kind=kOutput, calls=%fused_computation.9 | convolution fusion | flops 11821907968 | bytes 25690112 | tf_op jit(solution)/shard_map/dot_general | solution.py:38
  817.8 76.9 %reduce-scatter.5.cloned.1.call-done = bf16[256,2048]{1,0:T(8,128)(2,1)} async-done(((bf16[1024,2048]{1,0:T(8,128)(2,1)}), bf16[256,2048]{1,0:T(8,128)(2,1)}) %reduce-scatter.5.cloned.1.call-update) | async-done | bytes 1048592 | tf_op jit(solution)/shard_map/reduce_scatter | solution.py:69
  900.1 5.7 copy.37
  905.8 5.6 copy.38
  914.0 5.7 copy.40
  919.7 5.7 copy.41
  (68 shorter events, 34.9 us)
Async XLA Ops:
  7.2 49.5 %all-gather.8.cloned.1.call-start = ((), (), s32[]{:S(2)}) async-start(), calls=%async_computation.6 | async-start | bytes 7208960 | tf_op jit(solution)/shard_map/all_gather | solution.py:26
  10.5 91.8 %all-gather.10.cloned.1.call-start = ((), (), s32[]{:S(2)}) async-start(), calls=%async_computation.7 | async-start | bytes 7208960 | tf_op jit(solution)/shard_map/all_gather | solution.py:27
  62.3 5.6 copy-start.5
  62.3 133.1 %all-to-all-start = ((bf16[512,4,1408]{2,0,1:T(8,128)(2,1)}), bf16[512,4,1408]{2,0,1:T(8,128)(2,1)}, u32[]{:S(2)}, u32[]{:S(2)}) async-start(bf16[512,4,1408]{2,0,1:T(8,128)(2,1)} %bitcast.71), calls=%async_computation | async-start | bytes 11534336 | tf_op jit(solution)/shard_map/all_to_all | solution.py:31
  67.8 148.9 %all-gather.12.cloned.1.call-start = ((), (), s32[]{:S(2)}) async-start(), calls=%async_computation.8 | async-start | bytes 7208960 | tf_op jit(solution)/shard_map/all_gather | solution.py:28
  195.4 5.5 copy-start.7
  195.4 5.6 copy-start.3
  195.4 132.2 %all-to-all-start.1 = ((bf16[512,4,1408]{2,0,1:T(8,128)(2,1)}), bf16[512,4,1408]{2,0,1:T(8,128)(2,1)}, u32[]{:S(2)}, u32[]{:S(2)}) async-start(bf16[512,4,1408]{2,0,1:T(8,128)(2,1)} %bitcast.70), calls=%async_computation.1 | async-start | bytes 11534336 | tf_op jit(solution)/shard_map/all_to_all | solution.py:32
  200.9 147.9 %all-gather.16.cloned.1.call-start = ((), (), s32[]{:S(2)}) async-start(), calls=%async_computation.11 | async-start | bytes 7208960 | tf_op jit(solution)/shard_map/all_gather | solution.py:26
  205.0 278.6 %reduce-scatter.3.cloned.1.call-start = ((), (), s32[]{:S(2)}) async-start(), calls=%async_computation.9 | async-start | bytes 5242880 | tf_op jit(solution)/shard_map/reduce_scatter | solution.py:60
  348.2 226.7 %all-gather.18.cloned.1.call-start = ((), (), s32[]{:S(2)}) async-start(), calls=%async_computation.12 | async-start | bytes 7208960 | tf_op jit(solution)/shard_map/all_gather | solution.py:27
  354.5 226.1 %all-to-all-start.2 = ((bf16[512,4,1408]{2,0,1:T(8,128)(2,1)}), bf16[512,4,1408]{2,0,1:T(8,128)(2,1)}, u32[]{:S(2)}, u32[]{:S(2)}) async-start(bf16[512,4,1408]{2,0,1:T(8,128)(2,1)} %bitcast.69), calls=%async_computation.3 | async-start | bytes 11534336 | tf_op jit(solution)/shard_map/all_to_all | solution.py:31
  359.6 393.4 %all-gather.14.cloned.1.call-start = ((), (), s32[]{:S(2)}) async-start(), calls=%async_computation.10 | async-start | bytes 5242880 | tf_op jit(solution)/shard_map/all_gather | solution.py:67
  359.7 131.3 %copy-start.6 = (f32[1408,512]{1,0:T(8,128)S(1)}, f32[1408,512]{1,0:T(8,128)}, u32[]{:S(2)}) copy-start(f32[1408,512]{1,0:T(8,128)} %param.15) | copy-start | bytes 8650756
  483.7 4.3 copy-start.1
  490.8 306.4 %all-gather.20.cloned.1.call-start = ((), (), s32[]{:S(2)}) async-start(), calls=%async_computation.13 | async-start | bytes 7208960 | tf_op jit(solution)/shard_map/all_gather | solution.py:28
  580.6 216.6 %all-to-all-start.3 = ((bf16[512,4,1408]{2,0,1:T(8,128)(2,1)}), bf16[512,4,1408]{2,0,1:T(8,128)(2,1)}, u32[]{:S(2)}, u32[]{:S(2)}) async-start(bf16[512,4,1408]{2,0,1:T(8,128)(2,1)} %bitcast.72), calls=%async_computation.4 | async-start | bytes 11534336 | tf_op jit(solution)/shard_map/all_to_all | solution.py:32
  585.9 308.8 %reduce-scatter.5.cloned.1.call-start = ((), (), s32[]{:S(2)}) async-start(), calls=%async_computation.14 | async-start | bytes 5242880 | tf_op jit(solution)/shard_map/reduce_scatter | solution.py:69
  817.8 77.0 %copy-start = (bf16[256,2048]{1,0:T(8,128)(2,1)S(1)}, bf16[256,2048]{1,0:T(8,128)(2,1)}, u32[]{:S(2)}) copy-start(bf16[256,2048]{1,0:T(8,128)(2,1)} %multiply_convert_fusion.5) | copy-start | bytes 3145732
  894.7 3.8 copy-start.2
  896.6 14.9 %slice-start = ((s8[5767168]{0:T(1024)(128)(4,1)}), s8[4194304]{0:T(1024)(128)(4,1)S(1)}, s32[]{:S(2)}) async-start(s8[5767168]{0:T(1024)(128)(4,1)} %bitcast.73), calls=%async_computation.15 | async-start | bytes 8388608
  900.1 11.3 %slice-start.1 = ((s8[5767168]{0:T(1024)(128)(4,1)}), s8[1572864]{0:T(1024)(128)(4,1)S(1)}, s32[]{:S(2)}) async-start(s8[5767168]{0:T(1024)(128)(4,1)} %bitcast.73), calls=%async_computation.16 | async-start | bytes 3145728
  913.9 11.5 %slice-start.2 = ((s8[5767168]{0:T(1024)(128)(4,1)}), s8[4194304]{0:T(1024)(128)(4,1)S(1)}, s32[]{:S(2)}) async-start(s8[5767168]{0:T(1024)(128)(4,1)} %bitcast.75), calls=%async_computation.17 | async-start | bytes 8388608
  919.7 5.7 slice-start.3
  (1 other events, 3.3 us)
Sparse Core Ops, SparseCore 0:
  10.6 46.0 all-gather.7
  58.8 43.3 all-gather.9
  104.4 43.3 all-gather.11
  205.2 43.7 all-gather.15
  348.4 135.2 reduce-scatter.2
  485.7 89.2 all-gather.17
  577.1 175.8 all-gather.13
  755.1 42.0 all-gather.19
  817.9 76.7 reduce-scatter.4
where the time goes:
time: 935 us; the launch traced here: 934 us
  waiting for transfers between devices  760 us (81%)
  matrix products  64.5 us (7%)
  local copies, waits for them, and re-layouts  50.3 us (5%)
  other arithmetic  23.4 us (3%)
  starting transfers between devices  22.1 us (2%)
  between operations  14 us (1%)
    all_gather x1, waiting for transfers between devices, body(): lax.all_gather(normed_own, 'fs', axis=0, tiled=True)  167 us
    reduce_scatter x1, waiting for transfers between devices, body(): lax.psum_scatter(row_terms(hidden_one, down_one).astype(jnp.bfloat16), 'f...  124 us
    all_gather x2, waiting for transfers between devices, relay_weights(): lax.all_gather(up_proj, 'tp', axis=1, tiled=True)  116 us
    all_to_all x2, waiting for transfers between devices, relay_weights(): lax.all_to_all(up_rows, 'fs', split_axis=1, concat_axis=0, tiled=True)  111 us
    all_to_all x2, waiting for transfers between devices, relay_weights(): lax.all_to_all(gate_rows, 'fs', split_axis=1, concat_axis=0, tiled=True)  87.6 us
    reduce_scatter x1, waiting for transfers between devices, body(): lax.psum_scatter(row_terms(hidden_two, down_two).astype(jnp.bfloat16), 'f...  76.9 us
    all_gather x2, waiting for transfers between devices, relay_weights(): lax.all_gather(gate_proj, 'tp', axis=1, tiled=True)  44.9 us
    dot_general x2, matrix products, row_terms(): return jnp.dot(hidden, down_proj, preferred_element_type=jnp.float32)  41.1 us
  transfers between devices with their start and end apart: 13, of which 9 were waited for; matrix products, arithmetic and copies ran while one was open for 9% of the time, Pallas kernels for 0%

commit v1 on v0

v1 whole, which is shorter than its diff:
```python
import jax
import jax.numpy as jnp
from jax import lax
from jax.experimental import pallas as pl
from jax.experimental.pallas import tpu as pltpu
from jax.sharding import PartitionSpec as P

norm_eps = 1e-05
deep_alpha = 2.0**0.25
half_step = 0.5
every_axis = ("grp", "fs", "tp")


def plain_norm(values):
    row_mean = jnp.mean(values, axis=-1, keepdims=True)
    centred = values - row_mean
    variance = jnp.mean(centred * centred, axis=-1, keepdims=True)
    return centred * lax.rsqrt(variance + norm_eps)


def gated_hidden(inputs, gate_proj, up_proj):
    gate_act = jnp.dot(inputs, gate_proj, preferred_element_type=jnp.float32)
    up_act = jnp.dot(inputs, up_proj, preferred_element_type=jnp.float32)
    return (jax.nn.silu(gate_act) * up_act).astype(jnp.bfloat16)


def relay_plain(proj):
    rows = lax.all_gather(proj, "tp", axis=1, tiled=True)
    return lax.all_to_all(rows, "fs", split_axis=1, concat_axis=0, tiled=True)


def paired_mesh(sizes):
    return [sizes[name] for name in every_axis] == [2, 4, 4]


def move(value, target):
    groups, depth, width = (lax.axis_size(name) for name in every_axis)
    pairs = []
    for y in range(groups):
        for z in range(depth):
            for t in range(width):
                y2, z2, x2, c2 = target(y, z, t // 2, t % 2)
                pairs.append(((y * depth + z) * width + t, (y2 * depth + z2) * width + 2 * x2 + c2))
    return lax.ppermute(value, every_axis, pairs)


def swap_chip(value):
    return move(value, lambda y, z, x, c: (y, z, 1 - x, c))


def swap_group(value):
    return move(value, lambda y, z, x, c: (1 - y, z, x, c))


def swap_core(value):
    return move(value, lambda y, z, x, c: (y, z, x, 1 - c))


def plane_of(z, c, hop, depth):
    near = (z - hop) % depth
    return (near, 1 - c) if near % 2 == c else ((near - 1) % depth, c)


def planes_landed(z, c, hop, depth):
    step = (z + c + 1) % 2
    return (z + hop + step) % depth, (z + hop + 1 - step) % depth


def stack_landed(pieces, hops):
    rows, columns = pieces[0].shape

    def kernel(*refs):
        landed = refs[: len(pieces)]
        whole, held, arrived, left = refs[len(pieces) :]
        y, z, t = (lax.axis_index(name) for name in every_axis)
        depth, c = lax.axis_size("fs"), t % 2
        slots = []
        for hop in hops:
            for plane in planes_landed(z, c, hop, depth):
                slots += [plane * 2 + y, plane * 2 + 1 - y]
        loads = [
            pltpu.make_async_copy(piece, held.at[k], arrived.at[k])
            for k, piece in enumerate(landed)
        ]
        stores = [
            pltpu.make_async_copy(held.at[k], whole.at[slot], left.at[k])
            for k, slot in enumerate(slots)
        ]
        for load in loads:
            load.start()
        for load, store in zip(loads, stores):
            load.wait()
            store.start()
        for store in stores:
            store.wait()

    stacked = pl.pallas_call(
        kernel,
        out_shape=jax.ShapeDtypeStruct((len(pieces), rows, columns), pieces[0].dtype),
        in_specs=[pl.BlockSpec(memory_space=pl.ANY)] * len(pieces),
        out_specs=pl.BlockSpec(memory_space=pl.ANY),
        scratch_shapes=[
            pltpu.VMEM((len(pieces), rows, columns), pieces[0].dtype),
            pltpu.SemaphoreType.DMA((len(pieces),)),
            pltpu.SemaphoreType.DMA((len(pieces),)),
        ],
        name="stack_landed",
    )(*pieces)
    return stacked.reshape(len(pieces) * rows, columns)


def relay_paired(proj):
    depth = lax.axis_size("fs")
    y, z, t = (lax.axis_index(name) for name in every_axis)
    x, c = t // 2, t % 2
    rows = proj.shape[0] // 2
    own = lax.dynamic_slice_in_dim(proj, y * rows, rows, 0)
    other = swap_chip(own)
    hops = tuple(reversed(range(0, depth, 2)))
    pieces = []
    for hop in hops:
        near = (z - hop) % depth
        goes = jnp.where(near % 2 == c, near, (near - 1) % depth)
        piece = jnp.where(goes // 2 == x, own, other)

        def target(y, z, x, c, hop=hop):
            plane, core = plane_of(z, c, hop, depth)
            return (y, plane, x, core)

        mine = move(piece, target)
        theirs = swap_group(mine)
        mine_far = swap_core(mine)
        theirs_far = swap_core(theirs)
        pieces += [mine, theirs, mine_far, theirs_far]
    return stack_landed(pieces, hops)


def join_columns(pieces):
    rows, columns = pieces[0].shape

    def kernel(*refs):
        landed = refs[: len(pieces)]
        whole, held, arrived, left = refs[len(pieces) :]
        t = lax.axis_index("tp")
        x, c = t // 2, t % 2
        places = [2 * x + c, 2 * (1 - x) + c, 2 * x + 1 - c, 2 * (1 - x) + 1 - c]
        loads = [
            pltpu.make_async_copy(piece, held.at[k], arrived.at[k])
            for k, piece in enumerate(landed)
        ]
        stores = [
            pltpu.make_async_copy(
                held.at[k], whole.at[:, pl.ds(pl.multiple_of(place * columns, columns), columns)], left.at[k]
            )
            for k, place in enumerate(places)
        ]
        for load in loads:
            load.start()
        for load, store in zip(loads, stores):
            load.wait()
            store.start()
        for store in stores:
            store.wait()

    return pl.pallas_call(
        kernel,
        out_shape=jax.ShapeDtypeStruct((rows, len(pieces) * columns), pieces[0].dtype),
        in_specs=[pl.BlockSpec(memory_space=pl.ANY)] * len(pieces),
        out_specs=pl.BlockSpec(memory_space=pl.ANY),
        scratch_shapes=[
            pltpu.VMEM((len(pieces), rows, columns), pieces[0].dtype),
            pltpu.SemaphoreType.DMA((len(pieces),)),
            pltpu.SemaphoreType.DMA((len(pieces),)),
        ],
        name="join_columns",
    )(*pieces)


def columns_paired(proj):
    other = swap_chip(proj)
    beside = swap_core(proj)
    across = swap_core(other)
    return join_columns([proj, other, beside, across])


def columns_plain(proj):
    return lax.all_gather(proj, "tp", axis=1, tiled=True)


def swap_near(value):
    return move(value, lambda y, z, x, c: (y, z ^ 1, x, c))


def swap_far(value):
    return move(value, lambda y, z, x, c: (y, z ^ 2, x, c))


def row_terms(hidden, down_proj):
    return jnp.dot(hidden, down_proj, preferred_element_type=jnp.float32)


def scatter_paired(terms):
    joined = swap_near(terms[3])
    joined = joined.astype(jnp.float32) + terms[2].astype(jnp.float32)
    far = swap_far(joined.astype(jnp.bfloat16))
    near = swap_near(terms[1])
    return terms[0].astype(jnp.float32) + near.astype(jnp.float32) + far.astype(jnp.float32)


def gather_paired(block):
    far = swap_far(block)
    near = swap_near(block)
    last = swap_near(far)
    return jnp.concatenate([block, near, far, last], axis=0)


def paired_ffn(tokens, norm_gain, one, two):
    gate_one, up_one, down_one = one
    gate_two, up_two, down_two = two
    planes, parts = 4, 2
    z = lax.axis_index("fs")
    own_count = tokens.shape[0] // planes
    rows = own_count // parts

    def terms_of(inputs, gate_proj, up_proj, down_proj):
        hidden = gated_hidden(inputs, gate_proj, up_proj)
        terms = row_terms(hidden, down_proj).astype(jnp.bfloat16)
        return [terms[k * rows : (k + 1) * rows] for k in range(planes)]

    owned, sent = [], []
    for part in range(parts):
        blocks = [lax.dynamic_slice_in_dim(tokens, (z ^ k) * own_count + part * rows, rows, 0) for k in range(planes)]
        owned.append(blocks[0])
        sent.append(terms_of(jnp.concatenate(blocks, axis=0), gate_one, up_one, down_one))
    normed, again = [], []
    for part in range(parts):
        ffn_one = scatter_paired(sent[part])
        normed.append(
            plain_norm(
                deep_alpha * owned[part].astype(jnp.float32) + half_step * ffn_one
            ).astype(jnp.bfloat16)
        )
        inputs = gather_paired(normed[part])
        again.append(terms_of(inputs, gate_two, up_two, down_two))
    results = []
    for part in range(parts):
        ffn_two = scatter_paired(again[part])
        residual_two = deep_alpha * norm_gain * normed[part].astype(jnp.float32)
        results.append(plain_norm(residual_two + half_step * ffn_two).astype(jnp.bfloat16))
    return jnp.concatenate(results, axis=0)


def plain_ffn(tokens, norm_gain, one, two):
    gate_one, up_one, down_one = one
    gate_two, up_two, down_two = two
    own_count = tokens.shape[0] // lax.axis_size("fs")
    own_first = lax.axis_index("fs") * own_count
    hidden_one = gated_hidden(tokens, gate_one, up_one)
    own_tokens = lax.dynamic_slice_in_dim(tokens, own_first, own_count, 0)
    ffn_one = lax.psum_scatter(
        row_terms(hidden_one, down_one).astype(jnp.bfloat16), "fs", scatter_dimension=0, tiled=True
    ).astype(jnp.float32)
    normed_own = plain_norm(
        deep_alpha * own_tokens.astype(jnp.float32) + half_step * ffn_one
    ).astype(jnp.bfloat16)
    hidden_two = gated_hidden(
        lax.all_gather(normed_own, "fs", axis=0, tiled=True), gate_two, up_two
    )
    ffn_two = lax.psum_scatter(
        row_terms(hidden_two, down_two).astype(jnp.bfloat16), "fs", scatter_dimension=0, tiled=True
    ).astype(jnp.float32)
    residual_two = deep_alpha * norm_gain * normed_own.astype(jnp.float32)
    return plain_norm(residual_two + half_step * ffn_two).astype(jnp.bfloat16)


def body(prompt, gate_first, up_first, down_first, norm_gain, gate_second, up_second, down_second):
    paired = paired_mesh({name: lax.axis_size(name) for name in every_axis})
    relay = relay_paired if paired else relay_plain
    columns = columns_paired if paired else columns_plain
    fs_index = lax.axis_index("fs")
    row_block = gate_first.shape[0]
    gain_rows = lax.dynamic_slice_in_dim(norm_gain, fs_index * row_block, row_block, 0)
    up_one = relay(up_first.astype(jnp.bfloat16))
    gate_one = relay(gate_first.astype(jnp.bfloat16))
    down_one = columns(down_first.astype(jnp.bfloat16))
    up_two = relay((gain_rows[:, None] * up_second).astype(jnp.bfloat16))
    gate_two = relay((gain_rows[:, None] * gate_second).astype(jnp.bfloat16))
    down_two = columns(down_second.astype(jnp.bfloat16))
    tokens = prompt.reshape(-1, prompt.shape[-1])
    one, two = (gate_one, up_one, down_one), (gate_two, up_two, down_two)
    result = (paired_ffn if paired else plain_ffn)(tokens, norm_gain, one, two)
    return (
        result.reshape(1, result.shape[0], result.shape[-1]),
        gate_one,
        up_one,
        down_one,
        gate_two,
        up_two,
        down_two,
    )


def solution(mesh):
    placed = (
        P(("grp", "tp"), None, None),
        P("fs", "tp"),
        P("fs", "tp"),
        P("fs", "tp"),
        P(),
        P("fs", "tp"),
        P("fs", "tp"),
        P("fs", "tp"),
    )
    return jax.shard_map(
        body,
        mesh=mesh,
        in_specs=placed,
        out_specs=(
            P(("grp", "tp"), "fs", None),
            P("grp", "fs"),
            P("grp", "fs"),
            P("fs", "grp"),
            P("grp", "fs"),
            P("grp", "fs"),
            P("fs", "grp"),
        ),
        check_vma=False,
    )
```

time: 935 us -> 581 us (0.62); the launches traced: 934 us -> 571 us
  waiting for transfers between devices: 760 us -> 308 us
  starting transfers between devices: 22.1 us -> 98.1 us
  local copies, waits for them, and re-layouts: 50.3 us -> 14.9 us
  matrix products: 64.5 us -> 97.6 us
  Pallas kernels: 0 us -> 30 us
  between operations: 14 us -> 1.6 us
    all_gather x7 -> x0, waiting for transfers between devices: 360 us -> none  [the longest x1 167 us: body(): lax.all_gather(normed_own, 'fs', axis=0, tiled=True)]
    ppermute x0 -> x60, waiting for transfers between devices: none -> 308 us  [move(): return lax.ppermute(value, every_axis, pairs)]
    reduce_scatter x2 -> x0, waiting for transfers between devices: 201 us -> none  [the longest x1 124 us: body(): lax.psum_scatter(row_terms(hidden_one, down_one).astype(jnp.bfloat16), 'f...]
    all_to_all x4 -> x0, waiting for transfers between devices: 198 us -> none  [the longest x2 111 us: relay_weights(): lax.all_to_all(up_rows, 'fs', split_axis=1, concat_axis=0, tiled=True)]
    ppermute x0 -> x60, starting transfers between devices: none -> 98.1 us  [move(): return lax.ppermute(value, every_axis, pairs)]
    pallas_call x0 -> x6, Pallas kernels: none -> 30 us  [the longest x4 20.5 us: stack_landed(): pl.pallas_call(kernel, out_shape=jax.ShapeDtypeStruct((len(pieces), rows,...]
    unnamed x30 -> x56, local copies, waits for them, and re-layouts: 27.9 us -> 0.45 us
    dot_general x2 -> x4, matrix products: 41.1 us -> 65.2 us  [row_terms(): return jnp.dot(hidden, down_proj, preferred_element_type=jnp.float32)]
  transfers between devices with their start and end apart: 13 -> 60, of which waited for: 9 -> 23; matrix products, arithmetic and copies ran while one was open for 9% -> 22% of each run, Pallas kernels for 0% -> 5%
where the time goes in v1:
time: 581 us; the launch traced here: 571 us
  waiting for transfers between devices  308 us (53%)
  starting transfers between devices  98.1 us (17%)
  matrix products  97.6 us (17%)
  Pallas kernels  30 us (5%)
  other arithmetic  20.7 us (4%)
  local copies, waits for them, and re-layouts  14.9 us (3%)
    ppermute x60, waiting for transfers between devices, move(): return lax.ppermute(value, every_axis, pairs)  308 us
    ppermute x60, starting transfers between devices, move(): return lax.ppermute(value, every_axis, pairs)  98.1 us
    dot_general x4, matrix products, row_terms(): return jnp.dot(hidden, down_proj, preferred_element_type=jnp.float32)  65.2 us
    dot_general x4, matrix products, gated_hidden(): up_act = jnp.dot(inputs, up_proj, preferred_element_type=jnp.float32)  32.4 us
    pallas_call x4, Pallas kernels, stack_landed(): pl.pallas_call(kernel, out_shape=jax.ShapeDtypeStruct((len(pieces), rows,...  20.5 us
  transfers between devices with their start and end apart: 60, of which 23 were waited for; matrix products, arithmetic and copies ran while one was open for 22% of the time, Pallas kernels for 5%

profile of v1, /device:TPU:0, one launch (start us, length us, event | category | flops | bytes accessed | tf_op | source)
XLA Modules:
  0.0 570.5 jit_solution(3969709147966621282)
XLA Ops:
  11.5 11.7 %collective-permute-done.9 = bf16[256,1408]{1,0:T(8,128)(2,1)} collective-permute-done((bf16[256,1408]{1,0:T(8,128)(2,1)}, bf16[256,1408]{1,0:T(8,128)(2,1)}, u32[]{:S(2)}, u32[]{:S(2)}) %collective-permute-start.9) | collective-permute-done | bytes 720928 | tf_op jit(solution)/shard_map/ppermute | solution.py:44
  28.4 40.2 %collective-permute-done = bf16[256,1408]{1,0:T(8,128)(2,1)S(1)} collective-permute-done((bf16[256,1408]{1,0:T(8,128)(2,1)S(1)}, bf16[256,1408]{1,0:T(8,128)(2,1)S(1)}, u32[]{:S(2)}, u32[]{:S(2)}) %collective-permute-start) | collective-permute-done | bytes 720928 | tf_op jit(solution)/shard_map/ppermute | solution.py:44
  73.0 10.2 %collective-permute-done.5.refs_4_ = bf16[256,1408]{1,0:T(8,128)(2,1)} collective-permute-done((bf16[256,1408]{1,0:T(8,128)(2,1)S(1)}, bf16[256,1408]{1,0:T(8,128)(2,1)}, u32[]{:S(2)}, u32[]{:S(2)}) %collective-permute-start.5) | collective-permute-done | bytes 720928 | tf_op jit(solution)/shard_map/ppermute | solution.py:44
  85.0 13.9 %collective-permute-done.1.refs_0_ = bf16[256,1408]{1,0:T(8,128)(2,1)} collective-permute-done((bf16[256,1408]{1,0:T(8,128)(2,1)S(1)}, bf16[256,1408]{1,0:T(8,128)(2,1)}, u32[]{:S(2)}, u32[]{:S(2)}) %collective-permute-start.1) | collective-permute-done | bytes 720928 | tf_op jit(solution)/shard_map/ppermute | solution.py:44
  170.3 13.8 %convolution_convert_fusion.1 = bf16[512,2048]{1,0:T(8,128)(2,1)} fusion(bf16[1408,2048]{1,0:T(8,128)(2,1)} %join_columns.2, f32[512,1408]{1,0:T(8,128)} %fusion.8, bf16[2048,1408]{1,0:T(8,128)(2,1)} %bitcast.37, bf16[128,2048]{1,0:T(8,128)(2,1)} %get-tuple-element.17, bf16[128,2048]{1,0:T(8,128)(2,1)} %get-tuple-element.18, ...), kind=kOutput, calls=%fused_computation.1 | convolution fusion | flops 5919342592 | bytes 18612224 | tf_op jit(solution)/shard_map/dot_general | solution.py:199
  186.5 8.9 %collective-permute-start.52 = (bf16[128,2048]{1,0:T(8,128)(2,1)}, bf16[128,2048]{1,0:T(8,128)(2,1)}, u32[]{:S(2)}, u32[]{:S(2)}) collective-permute-start(bf16[128,2048]{1,0:T(8,128)(2,1)} %get-tuple-element.26), channel_id=1, source_target_pairs={{0,4},{1,5},{2,6},{3,7},{4,0},{5,1},{6,2},{7,3},{8,12},{9,13},{10,... | collective-permute-start | bytes 1572872 | tf_op jit(solution)/shard_map/ppermute | solution.py:44
  203.5 25.1 %convolution_convert_fusion.3 = bf16[512,2048]{1,0:T(8,128)(2,1)} fusion(bf16[1408,2048]{1,0:T(8,128)(2,1)} %join_columns.2, f32[512,1408]{1,0:T(8,128)} %fusion.12, bf16[2048,1408]{1,0:T(8,128)(2,1)} %bitcast.38, bf16[128,2048]{1,0:T(8,128)(2,1)} %get-tuple-element.14, bf16[128,2048]{1,0:T(8,128)(2,1)} %get-tuple-element.15, ...), kind=kOutput, calls=%fused_computation.3 | convolution fusion | flops 5919342592 | bytes 18612224 | tf_op jit(solution)/shard_map/dot_general | solution.py:199
  235.1 9.9 %collective-permute-done.22 = bf16[128,2048]{1,0:T(8,128)(2,1)S(1)} collective-permute-done((bf16[128,2048]{1,0:T(8,128)(2,1)S(1)}, bf16[128,2048]{1,0:T(8,128)(2,1)S(1)}, u32[]{:S(2)}, u32[]{:S(2)}) %collective-permute-start.22) | collective-permute-done | bytes 524320 | tf_op jit(solution)/shard_map/ppermute | solution.py:44
  246.0 14.4 %collective-permute-done.32.refs_4_ = bf16[256,1408]{1,0:T(8,128)(2,1)S(1)} collective-permute-done((bf16[256,1408]{1,0:T(8,128)(2,1)S(1)}, bf16[256,1408]{1,0:T(8,128)(2,1)S(1)}, u32[]{:S(2)}, u32[]{:S(2)}) %collective-permute-start.32) | collective-permute-done | bytes 720928 | tf_op jit(solution)/shard_map/ppermute | solution.py:44
  260.4 20.9 %collective-permute-done.51 = bf16[128,2048]{1,0:T(8,128)(2,1)S(1)} collective-permute-done((bf16[128,2048]{1,0:T(8,128)(2,1)S(1)}, bf16[128,2048]{1,0:T(8,128)(2,1)S(1)}, u32[]{:S(2)}, u32[]{:S(2)}) %collective-permute-start.51) | collective-permute-done | bytes 524320 | tf_op jit(solution)/shard_map/ppermute | solution.py:44
  287.2 26.1 %collective-permute-done.53 = bf16[128,2048]{1,0:T(8,128)(2,1)S(1)} collective-permute-done((bf16[128,2048]{1,0:T(8,128)(2,1)S(1)}, bf16[128,2048]{1,0:T(8,128)(2,1)S(1)}, u32[]{:S(2)}, u32[]{:S(2)}) %collective-permute-start.53) | collective-permute-done | bytes 524320 | tf_op jit(solution)/shard_map/ppermute | solution.py:44
  313.3 11.2 %collective-permute-done.23 = bf16[128,2048]{1,0:T(8,128)(2,1)S(1)} collective-permute-done((bf16[128,2048]{1,0:T(8,128)(2,1)S(1)}, bf16[128,2048]{1,0:T(8,128)(2,1)S(1)}, u32[]{:S(2)}, u32[]{:S(2)}) %collective-permute-start.23) | collective-permute-done | bytes 524320 | tf_op jit(solution)/shard_map/ppermute | solution.py:44
  325.4 26.3 %collective-permute-start.34 = (bf16[256,1408]{1,0:T(8,128)(2,1)S(1)}, bf16[256,1408]{1,0:T(8,128)(2,1)S(1)}, u32[]{:S(2)}, u32[]{:S(2)}) collective-permute-start(bf16[256,1408]{1,0:T(8,128)(2,1)S(1)} %collective-permute-done.32.refs_4_), channel_id=1, source_target_pairs={{0,1},{1,0},{2,3},{3,2},{4,5},{5,4},{6,7},{7,6},{8,9},{9,8},{10,11... | collective-permute-start | bytes 2162696 | tf_op jit(solution)/shard_map/ppermute | solution.py:44
  371.4 14.9 %collective-permute-done.29.refs_1_ = bf16[256,1408]{1,0:T(8,128)(2,1)S(1)} collective-permute-done((bf16[256,1408]{1,0:T(8,128)(2,1)S(1)}, bf16[256,1408]{1,0:T(8,128)(2,1)S(1)}, u32[]{:S(2)}, u32[]{:S(2)}) %collective-permute-start.29) | collective-permute-done | bytes 720928 | tf_op jit(solution)/shard_map/ppermute | solution.py:44
  388.4 13.4 %collective-permute-done.42.refs_5_ = bf16[256,1408]{1,0:T(8,128)(2,1)} collective-permute-done((bf16[256,1408]{1,0:T(8,128)(2,1)S(1)}, bf16[256,1408]{1,0:T(8,128)(2,1)}, u32[]{:S(2)}, u32[]{:S(2)}) %collective-permute-start.42) | collective-permute-done | bytes 720928 | tf_op jit(solution)/shard_map/ppermute | solution.py:44
  401.9 14.4 %collective-permute-done.38.refs_1_ = bf16[256,1408]{1,0:T(8,128)(2,1)} collective-permute-done((bf16[256,1408]{1,0:T(8,128)(2,1)S(1)}, bf16[256,1408]{1,0:T(8,128)(2,1)}, u32[]{:S(2)}, u32[]{:S(2)}) %collective-permute-start.38) | collective-permute-done | bytes 720928 | tf_op jit(solution)/shard_map/ppermute | solution.py:44
  417.6 17.0 %collective-permute-done.55 = bf16[128,2048]{1,0:T(8,128)(2,1)S(1)} collective-permute-done((bf16[128,2048]{1,0:T(8,128)(2,1)S(1)}, bf16[128,2048]{1,0:T(8,128)(2,1)S(1)}, u32[]{:S(2)}, u32[]{:S(2)}) %collective-permute-start.55) | collective-permute-done | bytes 524320 | tf_op jit(solution)/shard_map/ppermute | solution.py:44
  452.0 10.5 %collective-permute-done.56 = bf16[128,2048]{1,0:T(8,128)(2,1)} collective-permute-done((bf16[128,2048]{1,0:T(8,128)(2,1)S(1)}, bf16[128,2048]{1,0:T(8,128)(2,1)}, u32[]{:S(2)}, u32[]{:S(2)}) %collective-permute-start.56) | collective-permute-done | bytes 524320 | tf_op jit(solution)/shard_map/ppermute | solution.py:44
  470.2 12.5 %convolution_convert_fusion = bf16[512,2048]{1,0:T(8,128)(2,1)S(1)} fusion(bf16[1408,2048]{1,0:T(8,128)(2,1)} %join_columns.3, f32[512,1408]{1,0:T(8,128)} %fusion.6, bf16[2048,1408]{1,0:T(8,128)(2,1)} %bitcast.40, bf16[128,2048]{1,0:T(8,128)(2,1)} %collective-permute-done.56, bf16[128,2048]{1,0:T(8,128)(2,1)} %copy-done.26, bf16[128,2048]{1,0:T(8,128)(2,1)} %copy-done.27, ...), kind=kOutput, calls=%fused_computation | convolution fusion | flops 5919342592 | bytes 18612224 | tf_op jit(solution)/shard_map/dot_general | solution.py:199
  492.2 13.8 %convolution_convert_fusion.2 = bf16[512,2048]{1,0:T(8,128)(2,1)} fusion(bf16[1408,2048]{1,0:T(8,128)(2,1)} %join_columns.3, f32[512,1408]{1,0:T(8,128)} %fusion.10, bf16[2048,1408]{1,0:T(8,128)(2,1)} %bitcast.41, bf16[128,2048]{1,0:T(8,128)(2,1)} %collective-permute-done.26, bf16[128,2048]{1,0:T(8,128)(2,1)} %collective-permute-done.25, ...), kind=kOutput, calls=%fused_computation.2 | convolution fusion | flops 5919342592 | bytes 18612224 | tf_op jit(solution)/shard_map/dot_general | solution.py:199
  512.6 20.9 %collective-permute-done.49 = bf16[128,2048]{1,0:T(8,128)(2,1)S(1)} collective-permute-done((bf16[128,2048]{1,0:T(8,128)(2,1)S(1)}, bf16[128,2048]{1,0:T(8,128)(2,1)S(1)}, u32[]{:S(2)}, u32[]{:S(2)}) %collective-permute-start.49) | collective-permute-done | bytes 524320 | tf_op jit(solution)/shard_map/ppermute | solution.py:44
  533.8 15.9 %collective-permute-done.57 = bf16[128,2048]{1,0:T(8,128)(2,1)S(1)} collective-permute-done((bf16[128,2048]{1,0:T(8,128)(2,1)}, bf16[128,2048]{1,0:T(8,128)(2,1)S(1)}, u32[]{:S(2)}, u32[]{:S(2)}) %collective-permute-start.57) | collective-permute-done | bytes 524320 | tf_op jit(solution)/shard_map/ppermute | solution.py:44
  549.7 9.4 %collective-permute-done.48 = bf16[128,2048]{1,0:T(8,128)(2,1)S(1)} collective-permute-done((bf16[128,2048]{1,0:T(8,128)(2,1)S(1)}, bf16[128,2048]{1,0:T(8,128)(2,1)S(1)}, u32[]{:S(2)}, u32[]{:S(2)}) %collective-permute-start.48) | collective-permute-done | bytes 524320 | tf_op jit(solution)/shard_map/ppermute | solution.py:44
  559.0 8.3 %collective-permute-done.50 = bf16[128,2048]{1,0:T(8,128)(2,1)S(1)} collective-permute-done((bf16[128,2048]{1,0:T(8,128)(2,1)S(1)}, bf16[128,2048]{1,0:T(8,128)(2,1)S(1)}, u32[]{:S(2)}, u32[]{:S(2)}) %collective-permute-start.50) | collective-permute-done | bytes 524320 | tf_op jit(solution)/shard_map/ppermute | solution.py:44
  (205 shorter events, 185.3 us)
Async XLA Ops:
  7.9 63.9 %collective-permute-start.18 = (bf16[1408,512]{1,0:T(8,128)(2,1)S(1)}, bf16[1408,512]{1,0:T(8,128)(2,1)}, u32[]{:S(2)}, u32[]{:S(2)}) collective-permute-start(bf16[1408,512]{1,0:T(8,128)(2,1)S(1)} %convert_element_type.142.refs_0_), channel_id=1, source_target_pairs={{0,2},{1,3},{2,0},{3,1},{4,6},{5,7},{6,4},{7,5},{8,10},{9,11},{10,... | collective-permute-start | bytes 4325384 | tf_op jit(solution)/shard_map/ppermute | solution.py:44
  9.9 58.7 %collective-permute-start = (bf16[256,1408]{1,0:T(8,128)(2,1)S(1)}, bf16[256,1408]{1,0:T(8,128)(2,1)S(1)}, u32[]{:S(2)}, u32[]{:S(2)}) collective-permute-start(bf16[256,1408]{1,0:T(8,128)(2,1)S(1)} %dynamic-slice_convert_fusion.1), channel_id=1, source_target_pairs={{0,2},{1,3},{2,0},{3,1},{4,6},{5,7},{6,4},{7,5},{8,10},{9,11},{10,... | collective-permute-start | bytes 2162696 | tf_op jit(solution)/shard_map/ppermute | solution.py:44
  25.0 45.3 %collective-permute-start.14 = (bf16[256,1408]{1,0:T(8,128)(2,1)S(1)}, bf16[256,1408]{1,0:T(8,128)(2,1)}, u32[]{:S(2)}, u32[]{:S(2)}) collective-permute-start(bf16[256,1408]{1,0:T(8,128)(2,1)S(1)} %get-tuple-element.31), channel_id=1, source_target_pairs={{0,1},{1,13},{2,3},{3,15},{4,0},{5,4},{6,2},{7,6},{8,9},{9,5},{10,... | collective-permute-start | bytes 2162696 | tf_op jit(solution)/shard_map/ppermute | solution.py:44
  25.1 78.8 %collective-permute-start.19 = (bf16[1408,512]{1,0:T(8,128)(2,1)S(1)}, bf16[1408,512]{1,0:T(8,128)(2,1)}, u32[]{:S(2)}, u32[]{:S(2)}) collective-permute-start(bf16[1408,512]{1,0:T(8,128)(2,1)S(1)} %convert_element_type.142.refs_0_), channel_id=1, source_target_pairs={{0,1},{1,0},{2,3},{3,2},{4,5},{5,4},{6,7},{7,6},{8,9},{9,8},{10,11... | collective-permute-start | bytes 4325384 | tf_op jit(solution)/shard_map/ppermute | solution.py:44
  26.8 46.1 %collective-permute-start.10 = (bf16[256,1408]{1,0:T(8,128)(2,1)S(1)}, bf16[256,1408]{1,0:T(8,128)(2,1)}, u32[]{:S(2)}, u32[]{:S(2)}) collective-permute-start(bf16[256,1408]{1,0:T(8,128)(2,1)S(1)} %get-tuple-element.32), channel_id=1, source_target_pairs={{0,9},{1,5},{2,11},{3,7},{4,8},{5,12},{6,10},{7,14},{8,1},{9,13},{... | collective-permute-start | bytes 2162696 | tf_op jit(solution)/shard_map/ppermute | solution.py:44
  71.9 50.5 %collective-permute-start.20 = (bf16[1408,512]{1,0:T(8,128)(2,1)}, bf16[1408,512]{1,0:T(8,128)(2,1)}, u32[]{:S(2)}, u32[]{:S(2)}) collective-permute-start(bf16[1408,512]{1,0:T(8,128)(2,1)} %collective-permute-done.18.refs_1_), channel_id=1, source_target_pairs={{0,1},{1,0},{2,3},{3,2},{4,5},{5,4},{6,7},{7,6},{8,9},{9,8},{10,11... | collective-permute-start | bytes 4325384 | tf_op jit(solution)/shard_map/ppermute | solution.py:44
  108.9 36.3 %collective-permute-start.2 = (bf16[256,1408]{1,0:T(8,128)(2,1)}, bf16[256,1408]{1,0:T(8,128)(2,1)}, u32[]{:S(2)}, u32[]{:S(2)}) collective-permute-start(bf16[256,1408]{1,0:T(8,128)(2,1)} %collective-permute-done.1.refs_0_), channel_id=1, source_target_pairs={{0,16},{1,17},{2,18},{3,19},{4,20},{5,21},{6,22},{7,23},{8,24},{9,... | collective-permute-start | bytes 2162696 | tf_op jit(solution)/shard_map/ppermute | solution.py:44
  132.3 97.9 %collective-permute-start.27 = (bf16[256,1408]{1,0:T(8,128)(2,1)}, bf16[256,1408]{1,0:T(8,128)(2,1)}, u32[]{:S(2)}, u32[]{:S(2)}) collective-permute-start(bf16[256,1408]{1,0:T(8,128)(2,1)} %get-tuple-element.37), channel_id=1, source_target_pairs={{0,2},{1,3},{2,0},{3,1},{4,6},{5,7},{6,4},{7,5},{8,10},{9,11},{10,... | collective-permute-start | bytes 2162696 | tf_op jit(solution)/shard_map/ppermute | solution.py:44
  163.5 82.4 %collective-permute-start.36 = (bf16[256,1408]{1,0:T(8,128)(2,1)S(1)}, bf16[256,1408]{1,0:T(8,128)(2,1)}, u32[]{:S(2)}, u32[]{:S(2)}) collective-permute-start(bf16[256,1408]{1,0:T(8,128)(2,1)S(1)} %get-tuple-element.38), channel_id=1, source_target_pairs={{0,2},{1,3},{2,0},{3,1},{4,6},{5,7},{6,4},{7,5},{8,10},{9,11},{10,... | collective-permute-start | bytes 2162696 | tf_op jit(solution)/shard_map/ppermute | solution.py:44
  165.2 194.3 %collective-permute-start.46 = (bf16[1408,512]{1,0:T(8,128)(2,1)S(1)}, bf16[1408,512]{1,0:T(8,128)(2,1)}, u32[]{:S(2)}, u32[]{:S(2)}) collective-permute-start(bf16[1408,512]{1,0:T(8,128)(2,1)S(1)} %copy-done.1), channel_id=1, source_target_pairs={{0,1},{1,0},{2,3},{3,2},{4,5},{5,4},{6,7},{7,6},{8,9},{9,8},{10,11... | collective-permute-start | bytes 4325384 | tf_op jit(solution)/shard_map/ppermute | solution.py:44
  186.5 45.7 %collective-permute-start.52 = (bf16[128,2048]{1,0:T(8,128)(2,1)}, bf16[128,2048]{1,0:T(8,128)(2,1)}, u32[]{:S(2)}, u32[]{:S(2)}) collective-permute-start(bf16[128,2048]{1,0:T(8,128)(2,1)} %get-tuple-element.26), channel_id=1, source_target_pairs={{0,4},{1,5},{2,6},{3,7},{4,0},{5,1},{6,2},{7,3},{8,12},{9,13},{10,... | collective-permute-start | bytes 1572872 | tf_op jit(solution)/shard_map/ppermute | solution.py:44
  232.1 49.2 %collective-permute-start.51 = (bf16[128,2048]{1,0:T(8,128)(2,1)S(1)}, bf16[128,2048]{1,0:T(8,128)(2,1)S(1)}, u32[]{:S(2)}, u32[]{:S(2)}) collective-permute-start(bf16[128,2048]{1,0:T(8,128)(2,1)S(1)} %copy-done.24), channel_id=1, source_target_pairs={{0,4},{1,5},{2,6},{3,7},{4,0},{5,1},{6,2},{7,3},{8,12},{9,13},{10,... | collective-permute-start | bytes 1572872 | tf_op jit(solution)/shard_map/ppermute | solution.py:44
  245.0 116.0 %collective-permute-start.45 = (bf16[1408,512]{1,0:T(8,128)(2,1)S(1)}, bf16[1408,512]{1,0:T(8,128)(2,1)S(1)}, u32[]{:S(2)}, u32[]{:S(2)}) collective-permute-start(bf16[1408,512]{1,0:T(8,128)(2,1)S(1)} %copy-done.1), channel_id=1, source_target_pairs={{0,2},{1,3},{2,0},{3,1},{4,6},{5,7},{6,4},{7,5},{8,10},{9,11},{10,... | collective-permute-start | bytes 4325384 | tf_op jit(solution)/shard_map/ppermute | solution.py:44
  245.9 41.3 %collective-permute-start.21 = (bf16[128,2048]{1,0:T(8,128)(2,1)S(1)}, bf16[128,2048]{1,0:T(8,128)(2,1)S(1)}, u32[]{:S(2)}, u32[]{:S(2)}) collective-permute-start(bf16[128,2048]{1,0:T(8,128)(2,1)S(1)} %get-tuple-element.21), channel_id=1, source_target_pairs={{0,4},{1,5},{2,6},{3,7},{4,0},{5,1},{6,2},{7,3},{8,12},{9,13},{10,... | collective-permute-start | bytes 1572872 | tf_op jit(solution)/shard_map/ppermute | solution.py:44
  260.4 52.8 %collective-permute-start.53 = (bf16[128,2048]{1,0:T(8,128)(2,1)S(1)}, bf16[128,2048]{1,0:T(8,128)(2,1)S(1)}, u32[]{:S(2)}, u32[]{:S(2)}) collective-permute-start(bf16[128,2048]{1,0:T(8,128)(2,1)S(1)} %add_convert_fusion.1), channel_id=1, source_target_pairs={{0,8},{1,9},{2,10},{3,11},{4,12},{5,13},{6,14},{7,15},{8,0},{9,1},... | collective-permute-start | bytes 1572872 | tf_op jit(solution)/shard_map/ppermute | solution.py:44
  281.3 43.2 %collective-permute-start.23 = (bf16[128,2048]{1,0:T(8,128)(2,1)S(1)}, bf16[128,2048]{1,0:T(8,128)(2,1)S(1)}, u32[]{:S(2)}, u32[]{:S(2)}) collective-permute-start(bf16[128,2048]{1,0:T(8,128)(2,1)S(1)} %add_convert_fusion.3), channel_id=1, source_target_pairs={{0,8},{1,9},{2,10},{3,11},{4,12},{5,13},{6,14},{7,15},{8,0},{9,1},... | collective-permute-start | bytes 1572872 | tf_op jit(solution)/shard_map/ppermute | solution.py:44
  287.2 38.2 %collective-permute-start.28 = (bf16[256,1408]{1,0:T(8,128)(2,1)S(1)}, bf16[256,1408]{1,0:T(8,128)(2,1)S(1)}, u32[]{:S(2)}, u32[]{:S(2)}) collective-permute-start(bf16[256,1408]{1,0:T(8,128)(2,1)S(1)} %get-tuple-element.28), channel_id=1, source_target_pairs={{0,9},{1,5},{2,11},{3,7},{4,8},{5,12},{6,10},{7,14},{8,1},{9,13},{... | collective-permute-start | bytes 2162696 | tf_op jit(solution)/shard_map/ppermute | solution.py:44
  313.3 38.5 %collective-permute-start.41 = (bf16[256,1408]{1,0:T(8,128)(2,1)S(1)}, bf16[256,1408]{1,0:T(8,128)(2,1)S(1)}, u32[]{:S(2)}, u32[]{:S(2)}) collective-permute-start(bf16[256,1408]{1,0:T(8,128)(2,1)S(1)} %get-tuple-element.33), channel_id=1, source_target_pairs={{0,1},{1,13},{2,3},{3,15},{4,0},{5,4},{6,2},{7,6},{8,9},{9,5},{10,... | collective-permute-start | bytes 2162696 | tf_op jit(solution)/shard_map/ppermute | solution.py:44
  325.4 36.6 %collective-permute-start.34 = (bf16[256,1408]{1,0:T(8,128)(2,1)S(1)}, bf16[256,1408]{1,0:T(8,128)(2,1)S(1)}, u32[]{:S(2)}, u32[]{:S(2)}) collective-permute-start(bf16[256,1408]{1,0:T(8,128)(2,1)S(1)} %collective-permute-done.32.refs_4_), channel_id=1, source_target_pairs={{0,1},{1,0},{2,3},{3,2},{4,5},{5,4},{6,7},{7,6},{8,9},{9,8},{10,11... | collective-permute-start | bytes 2162696 | tf_op jit(solution)/shard_map/ppermute | solution.py:44
  362.0 39.8 %collective-permute-start.42 = (bf16[256,1408]{1,0:T(8,128)(2,1)S(1)}, bf16[256,1408]{1,0:T(8,128)(2,1)}, u32[]{:S(2)}, u32[]{:S(2)}) collective-permute-start(bf16[256,1408]{1,0:T(8,128)(2,1)S(1)} %collective-permute-done.41.refs_4_), channel_id=1, source_target_pairs={{0,16},{1,17},{2,18},{3,19},{4,20},{5,21},{6,22},{7,23},{8,24},{9,... | collective-permute-start | bytes 2162696 | tf_op jit(solution)/shard_map/ppermute | solution.py:44
  370.9 46.7 %collective-permute-start.47 = (bf16[1408,512]{1,0:T(8,128)(2,1)S(1)}, bf16[1408,512]{1,0:T(8,128)(2,1)S(1)}, u32[]{:S(2)}, u32[]{:S(2)}) collective-permute-start(bf16[1408,512]{1,0:T(8,128)(2,1)S(1)} %collective-permute-done.45.refs_1_), channel_id=1, source_target_pairs={{0,1},{1,0},{2,3},{3,2},{4,5},{5,4},{6,7},{7,6},{8,9},{9,8},{10,11... | collective-permute-start | bytes 4325384 | tf_op jit(solution)/shard_map/ppermute | solution.py:44
  509.4 40.3 %collective-permute-start.57 = (bf16[128,2048]{1,0:T(8,128)(2,1)}, bf16[128,2048]{1,0:T(8,128)(2,1)S(1)}, u32[]{:S(2)}, u32[]{:S(2)}) collective-permute-start(bf16[128,2048]{1,0:T(8,128)(2,1)} %get-tuple-element.23), channel_id=1, source_target_pairs={{0,4},{1,5},{2,6},{3,7},{4,0},{5,1},{6,2},{7,3},{8,12},{9,13},{10,... | collective-permute-start | bytes 1572872 | tf_op jit(solution)/shard_map/ppermute | solution.py:44
  509.5 49.5 %collective-permute-start.48 = (bf16[128,2048]{1,0:T(8,128)(2,1)S(1)}, bf16[128,2048]{1,0:T(8,128)(2,1)S(1)}, u32[]{:S(2)}, u32[]{:S(2)}) collective-permute-start(bf16[128,2048]{1,0:T(8,128)(2,1)S(1)} %get-tuple-element.19), channel_id=1, source_target_pairs={{0,4},{1,5},{2,6},{3,7},{4,0},{5,1},{6,2},{7,3},{8,12},{9,13},{10,... | collective-permute-start | bytes 1572872 | tf_op jit(solution)/shard_map/ppermute | solution.py:44
  512.6 46.5 %collective-permute-start.59 = (bf16[128,2048]{1,0:T(8,128)(2,1)S(1)}, bf16[128,2048]{1,0:T(8,128)(2,1)S(1)}, u32[]{:S(2)}, u32[]{:S(2)}) collective-permute-start(bf16[128,2048]{1,0:T(8,128)(2,1)S(1)} %add_convert_fusion), channel_id=1, source_target_pairs={{0,8},{1,9},{2,10},{3,11},{4,12},{5,13},{6,14},{7,15},{8,0},{9,1},... | collective-permute-start | bytes 1572872 | tf_op jit(solution)/shard_map/ppermute | solution.py:44
  (64 other events, 1753.3 us)

commit v2 on v1

--- a/solution.py
+++ b/solution.py
@@ -24,9 +24,9 @@
     return (jax.nn.silu(gate_act) * up_act).astype(jnp.bfloat16)
 
 
-def relay_plain(proj):
-    rows = lax.all_gather(proj, "tp", axis=1, tiled=True)
-    return lax.all_to_all(rows, "fs", split_axis=1, concat_axis=0, tiled=True)
+def relay_plain(*projs):
+    rows = [lax.all_gather(proj, "tp", axis=1, tiled=True) for proj in projs]
+    return [lax.all_to_all(part, "fs", split_axis=1, concat_axis=0, tiled=True) for part in rows]
 
 
 def paired_mesh(sizes):
@@ -67,11 +67,11 @@
 
 
 def stack_landed(pieces, hops):
-    rows, columns = pieces[0].shape
+    count, rows, columns = pieces[0].shape
 
     def kernel(*refs):
-        landed = refs[: len(pieces)]
-        whole, held, arrived, left = refs[len(pieces) :]
+        landed, wholes = refs[: len(pieces)], refs[len(pieces) : len(pieces) + count]
+        held, arrived, left = refs[len(pieces) + count :]
         y, z, t = (lax.axis_index(name) for name in every_axis)
         depth, c = lax.axis_size("fs"), t % 2
         slots = []
@@ -83,38 +83,43 @@
             for k, piece in enumerate(landed)
         ]
         stores = [
-            pltpu.make_async_copy(held.at[k], whole.at[slot], left.at[k])
+            [
+                pltpu.make_async_copy(held.at[k, i], whole.at[slot], left.at[i, k])
+                for i, whole in enumerate(wholes)
+            ]
             for k, slot in enumerate(slots)
         ]
         for load in loads:
             load.start()
-        for load, store in zip(loads, stores):
+        for load, outs in zip(loads, stores):
             load.wait()
-            store.start()
-        for store in stores:
-            store.wait()
+            for out in outs:
+                out.start()
+        for outs in stores:
+            for out in outs:
+                out.wait()
 
     stacked = pl.pallas_call(
         kernel,
-        out_shape=jax.ShapeDtypeStruct((len(pieces), rows, columns), pieces[0].dtype),
+        out_shape=[jax.ShapeDtypeStruct((len(pieces), rows, columns), pieces[0].dtype)] * count,
         in_specs=[pl.BlockSpec(memory_space=pl.ANY)] * len(pieces),
-        out_specs=pl.BlockSpec(memory_space=pl.ANY),
+        out_specs=[pl.BlockSpec(memory_space=pl.ANY)] * count,
         scratch_shapes=[
-            pltpu.VMEM((len(pieces), rows, columns), pieces[0].dtype),
+            pltpu.VMEM((len(pieces), count, rows, columns), pieces[0].dtype),
             pltpu.SemaphoreType.DMA((len(pieces),)),
-            pltpu.SemaphoreType.DMA((len(pieces),)),
+            pltpu.SemaphoreType.DMA((count, len(pieces))),
         ],
         name="stack_landed",
     )(*pieces)
-    return stacked.reshape(len(pieces) * rows, columns)
-
-
-def relay_paired(proj):
+    return [whole.reshape(len(pieces) * rows, columns) for whole in stacked]
+
+
+def relay_paired(*projs):
     depth = lax.axis_size("fs")
     y, z, t = (lax.axis_index(name) for name in every_axis)
     x, c = t // 2, t % 2
-    rows = proj.shape[0] // 2
-    own = lax.dynamic_slice_in_dim(proj, y * rows, rows, 0)
+    rows = projs[0].shape[0] // 2
+    own = jnp.stack([lax.dynamic_slice_in_dim(proj, y * rows, rows, 0) for proj in projs])
     other = swap_chip(own)
     hops = tuple(reversed(range(0, depth, 2)))
     pieces = []
@@ -217,23 +222,27 @@
 def paired_ffn(tokens, norm_gain, one, two):
     gate_one, up_one, down_one = one
     gate_two, up_two, down_two = two
-    planes, parts = 4, 2
-    z = lax.axis_index("fs")
+    planes, z = 4, lax.axis_index("fs")
     own_count = tokens.shape[0] // planes
-    rows = own_count // parts
+    later = own_count // 2
+    spans = ((0, own_count - later), (own_count - later, later))
 
     def terms_of(inputs, gate_proj, up_proj, down_proj):
+        rows = inputs.shape[0] // planes
         hidden = gated_hidden(inputs, gate_proj, up_proj)
-        terms = row_terms(hidden, down_proj).astype(jnp.bfloat16)
+        terms = row_terms(lax.optimization_barrier(hidden), down_proj).astype(jnp.bfloat16)
         return [terms[k * rows : (k + 1) * rows] for k in range(planes)]
 
     owned, sent = [], []
-    for part in range(parts):
-        blocks = [lax.dynamic_slice_in_dim(tokens, (z ^ k) * own_count + part * rows, rows, 0) for k in range(planes)]
+    for start, rows in spans:
+        blocks = [
+            lax.dynamic_slice_in_dim(tokens, (z ^ k) * own_count + start, rows, 0)
+            for k in range(planes)
+        ]
         owned.append(blocks[0])
         sent.append(terms_of(jnp.concatenate(blocks, axis=0), gate_one, up_one, down_one))
     normed, again = [], []
-    for part in range(parts):
+    for part in range(len(spans)):
         ffn_one = scatter_paired(sent[part])
         normed.append(
             plain_norm(
@@ -243,7 +252,7 @@
         inputs = gather_paired(normed[part])
         again.append(terms_of(inputs, gate_two, up_two, down_two))
     results = []
-    for part in range(parts):
+    for part in range(len(spans)):
         ffn_two = scatter_paired(again[part])
         residual_two = deep_alpha * norm_gain * normed[part].astype(jnp.float32)
         results.append(plain_norm(residual_two + half_step * ffn_two).astype(jnp.bfloat16))
@@ -280,11 +289,13 @@
     fs_index = lax.axis_index("fs")
     row_block = gate_first.shape[0]
     gain_rows = lax.dynamic_slice_in_dim(norm_gain, fs_index * row_block, row_block, 0)
-    up_one = relay(up_first.astype(jnp.bfloat16))
-    gate_one = relay(gate_first.astype(jnp.bfloat16))
+    (gate_one,) = relay(gate_first.astype(jnp.bfloat16))
+    (up_one,) = relay(up_first.astype(jnp.bfloat16))
     down_one = columns(down_first.astype(jnp.bfloat16))
-    up_two = relay((gain_rows[:, None] * up_second).astype(jnp.bfloat16))
-    gate_two = relay((gain_rows[:, None] * gate_second).astype(jnp.bfloat16))
+    up_two, gate_two = relay(
+        (gain_rows[:, None] * up_second).astype(jnp.bfloat16),
+        (gain_rows[:, None] * gate_second).astype(jnp.bfloat16),
+    )
     down_two = columns(down_second.astype(jnp.bfloat16))
     tokens = prompt.reshape(-1, prompt.shape[-1])
     one, two = (gate_one, up_one, down_one), (gate_two, up_two, down_two)

time: 581 us -> 468 us (0.81); the launches traced: 571 us -> 467 us
  waiting for transfers between devices: 308 us -> 261 us
  matrix products: 97.6 us -> 62.9 us
  starting transfers between devices: 98.1 us -> 86.7 us
    dot_general x4, matrix products: 65.2 us -> 18 us  [row_terms(): return jnp.dot(hidden, down_proj, preferred_element_type=jnp.float32)]
    ppermute x60 -> x51, waiting for transfers between devices: 308 us -> 261 us  [move(): return lax.ppermute(value, every_axis, pairs)]
    dot_general x0 -> x4, matrix products: none -> 24.3 us  [gated_hidden(): gate_act = jnp.dot(inputs, gate_proj, preferred_element_type=jnp.float32)]
    dot_general x4, matrix products: 32.4 us -> 20.6 us  [gated_hidden(): up_act = jnp.dot(inputs, up_proj, preferred_element_type=jnp.float32)]
    ppermute x60 -> x51, starting transfers between devices: 98.1 us -> 86.7 us  [move(): return lax.ppermute(value, every_axis, pairs)]
    slice x4, local copies, waits for them, and re-layouts: 6.23 us -> 0.39 us  [terms_of(): return [terms[k * rows:(k + 1) * rows] for k in range(planes)]]
    pallas_call x4 -> x3, Pallas kernels: 20.5 us -> 19 us  [stack_landed(): pl.pallas_call(kernel, out_shape=[jax.ShapeDtypeStruct((len(pieces), rows...]
  transfers between devices with their start and end apart: 60 -> 51, of which waited for: 23 -> 21; matrix products, arithmetic and copies ran while one was open for 22% -> 18% of each run, Pallas kernels for 5% -> 6%
where the time goes in v2:
time: 468 us; the launch traced here: 467 us
  waiting for transfers between devices  261 us (56%)
  starting transfers between devices  86.7 us (19%)
  matrix products  62.9 us (13%)
  Pallas kernels  28.4 us (6%)
  other arithmetic  16.2 us (3%)
  local copies, waits for them, and re-layouts  10.6 us (2%)
    ppermute x51, waiting for transfers between devices, move(): return lax.ppermute(value, every_axis, pairs)  261 us
    ppermute x51, starting transfers between devices, move(): return lax.ppermute(value, every_axis, pairs)  86.7 us
    dot_general x4, matrix products, gated_hidden(): gate_act = jnp.dot(inputs, gate_proj, preferred_element_type=jnp.float32)  24.3 us
    dot_general x4, matrix products, gated_hidden(): up_act = jnp.dot(inputs, up_proj, preferred_element_type=jnp.float32)  20.6 us
    pallas_call x3, Pallas kernels, stack_landed(): pl.pallas_call(kernel, out_shape=[jax.ShapeDtypeStruct((len(pieces), rows...  19 us
    dot_general x4, matrix products, row_terms(): return jnp.dot(hidden, down_proj, preferred_element_type=jnp.float32)  18 us
    pallas_call x2, Pallas kernels, join_columns(): pl.pallas_call(kernel, out_shape=jax.ShapeDtypeStruct((rows, len(pieces)...  9.38 us
  transfers between devices with their start and end apart: 51, of which 21 were waited for; matrix products, arithmetic and copies ran while one was open for 18% of the time, Pallas kernels for 6%

profile of v2, /device:TPU:0, one launch (start us, length us, event | category | flops | bytes accessed | tf_op | source)
XLA Modules:
  0.0 467.4 jit_solution(14185193144811835903)
XLA Ops:
  10.4 12.8 %collective-permute-done = bf16[1,256,1408]{2,1,0:T(8,128)(2,1)} collective-permute-done((bf16[1,256,1408]{2,1,0:T(8,128)(2,1)}, bf16[1,256,1408]{2,1,0:T(8,128)(2,1)}, u32[]{:S(2)}, u32[]{:S(2)}) %collective-permute-start) | collective-permute-done | bytes 720928 | tf_op jit(solution)/shard_map/ppermute | solution.py:44
  27.4 11.2 %collective-permute-done.9 = bf16[1,256,1408]{2,1,0:T(8,128)(2,1)S(1)} collective-permute-done((bf16[1,256,1408]{2,1,0:T(8,128)(2,1)S(1)}, bf16[1,256,1408]{2,1,0:T(8,128)(2,1)S(1)}, u32[]{:S(2)}, u32[]{:S(2)}) %collective-permute-start.9) | collective-permute-done | bytes 720928 | tf_op jit(solution)/shard_map/ppermute | solution.py:44
  48.8 20.4 %collective-permute-done.10.refs_0_ = bf16[1,256,1408]{2,1,0:T(8,128)(2,1)S(1)} collective-permute-done((bf16[1,256,1408]{2,1,0:T(8,128)(2,1)S(1)}, bf16[1,256,1408]{2,1,0:T(8,128)(2,1)S(1)}, u32[]{:S(2)}, u32[]{:S(2)}) %collective-permute-start.10) | collective-permute-done | bytes 720928 | tf_op jit(solution)/shard_map/ppermute | solution.py:44
  69.2 21.3 %collective-permute-start.3 = (bf16[1,256,1408]{2,1,0:T(8,128)(2,1)}, bf16[1,256,1408]{2,1,0:T(8,128)(2,1)}, u32[]{:S(2)}, u32[]{:S(2)}) collective-permute-start(bf16[1,256,1408]{2,1,0:T(8,128)(2,1)} %collective-permute-done.1.refs_0_), channel_id=1, source_target_pairs={{0,1},{1,0},{2,3},{3,2},{4,5},{5,4},{6,7},{7,6},{8,9},{9,8},{10,11... | collective-permute-start | bytes 2162696 | tf_op jit(solution)/shard_map/ppermute | solution.py:44
  110.4 16.9 %collective-permute-done.18.refs_1_ = bf16[1408,512]{1,0:T(8,128)(2,1)} collective-permute-done((bf16[1408,512]{1,0:T(8,128)(2,1)}, bf16[1408,512]{1,0:T(8,128)(2,1)}, u32[]{:S(2)}, u32[]{:S(2)}) %collective-permute-start.18) | collective-permute-done | bytes 1441824 | tf_op jit(solution)/shard_map/ppermute | solution.py:44
  128.8 8.2 %fusion.9 = f32[512,1408]{1,0:T(8,128)} fusion(bf16[2048,1408]{1,0:T(8,128)(2,1)} %bitcast.50, bf16[128,2048]{1,0:T(8,128)(2,1)} %get-tuple-element.21, bf16[128,2048]{1,0:T(8,128)(2,1)} %get-tuple-element.22, bf16[128,2048]{1,0:T(8,128)(2,1)} %get-tuple-element.16, bf16[128,2048]{1,0:T(8,128)(2,1)S(1)} %get-tuple-element.17), kind=kOutput, calls=%fused_computation.57 | convolution fusion | flops 2961178624 | bytes 10747904 | tf_op jit(solution)/shard_map/dot_general | solution.py:22
  143.1 9.3 %collective-permute-start.32 = (bf16[2,256,1408]{2,1,0:T(8,128)(2,1)}, bf16[2,256,1408]{2,1,0:T(8,128)(2,1)}, u32[]{:S(2)}, u32[]{:S(2)}) collective-permute-start(bf16[2,256,1408]{2,1,0:T(8,128)(2,1)} %get-tuple-element.23), channel_id=1, source_target_pairs={{0,1},{1,13},{2,3},{3,15},{4,0},{5,4},{6,2},{7,6},{8,9},{9,5},{10,... | collective-permute-start | bytes 4325384 | tf_op jit(solution)/shard_map/ppermute | solution.py:44
  157.6 8.6 %multiply_convert_fusion.1 = bf16[512,1408]{1,0:T(8,128)(2,1)} fusion(f32[512,1408]{1,0:T(8,128)} %fusion.9, bf16[2048,1408]{1,0:T(8,128)(2,1)} %bitcast.53, bf16[128,2048]{1,0:T(8,128)(2,1)} %get-tuple-element.21, bf16[128,2048]{1,0:T(8,128)(2,1)} %get-tuple-element.22, bf16[128,2048]{1,0:T(8,128)(2,1)} %get-tuple-element.16, ...), kind=kOutput, calls=%fused_computation.5 | convolution fusion | flops 2965504000 | bytes 12189696 | tf_op jit(solution)/shard_map/dot_general | solution.py:23
  170.9 6.6 %convolution_convert_fusion.1 = bf16[512,2048]{1,0:T(8,128)(2,1)S(1)} fusion(bf16[512,1408]{1,0:T(8,128)(2,1)} %multiply_convert_fusion.1, bf16[1408,2048]{1,0:T(8,128)(2,1)} %join_columns.2), kind=kOutput, calls=%fused_computation.1 | convolution fusion | flops 2953838592 | bytes 9306112 | tf_op jit(solution)/shard_map/dot_general | solution.py:204
  198.1 14.8 %collective-permute-done.42 = bf16[128,2048]{1,0:T(8,128)(2,1)S(1)} collective-permute-done((bf16[128,2048]{1,0:T(8,128)(2,1)S(1)}, bf16[128,2048]{1,0:T(8,128)(2,1)S(1)}, u32[]{:S(2)}, u32[]{:S(2)}) %collective-permute-start.42) | collective-permute-done | bytes 524320 | tf_op jit(solution)/shard_map/ppermute | solution.py:44
  217.9 9.9 %collective-permute-done.22 = bf16[128,2048]{1,0:T(8,128)(2,1)S(1)} collective-permute-done((bf16[128,2048]{1,0:T(8,128)(2,1)S(1)}, bf16[128,2048]{1,0:T(8,128)(2,1)S(1)}, u32[]{:S(2)}, u32[]{:S(2)}) %collective-permute-start.22) | collective-permute-done | bytes 524320 | tf_op jit(solution)/shard_map/ppermute | solution.py:44
  230.3 8.0 %collective-permute-done.44 = bf16[128,2048]{1,0:T(8,128)(2,1)S(1)} collective-permute-done((bf16[128,2048]{1,0:T(8,128)(2,1)S(1)}, bf16[128,2048]{1,0:T(8,128)(2,1)S(1)}, u32[]{:S(2)}, u32[]{:S(2)}) %collective-permute-start.44) | collective-permute-done | bytes 524320 | tf_op jit(solution)/shard_map/ppermute | solution.py:44
  247.0 14.2 %collective-permute-done.21 = bf16[128,2048]{1,0:T(8,128)(2,1)S(1)} collective-permute-done((bf16[128,2048]{1,0:T(8,128)(2,1)S(1)}, bf16[128,2048]{1,0:T(8,128)(2,1)S(1)}, u32[]{:S(2)}, u32[]{:S(2)}) %collective-permute-start.21) | collective-permute-done | bytes 524320 | tf_op jit(solution)/shard_map/ppermute | solution.py:44
  269.4 8.7 %collective-permute-done.29.refs_1_ = bf16[2,256,1408]{2,1,0:T(8,128)(2,1)} collective-permute-done((bf16[2,256,1408]{2,1,0:T(8,128)(2,1)}, bf16[2,256,1408]{2,1,0:T(8,128)(2,1)}, u32[]{:S(2)}, u32[]{:S(2)}) %collective-permute-start.29) | collective-permute-done | bytes 1441824 | tf_op jit(solution)/shard_map/ppermute | solution.py:44
  280.5 28.5 %collective-permute-done.33.refs_5_ = bf16[2,256,1408]{2,1,0:T(8,128)(2,1)} collective-permute-done((bf16[2,256,1408]{2,1,0:T(8,128)(2,1)}, bf16[2,256,1408]{2,1,0:T(8,128)(2,1)}, u32[]{:S(2)}, u32[]{:S(2)}) %collective-permute-start.33) | collective-permute-done | bytes 1441824 | tf_op jit(solution)/shard_map/ppermute | solution.py:44
  314.1 33.2 %collective-permute-done.46 = bf16[128,2048]{1,0:T(8,128)(2,1)S(1)} collective-permute-done((bf16[128,2048]{1,0:T(8,128)(2,1)S(1)}, bf16[128,2048]{1,0:T(8,128)(2,1)S(1)}, u32[]{:S(2)}, u32[]{:S(2)}) %collective-permute-start.46) | collective-permute-done | bytes 524320 | tf_op jit(solution)/shard_map/ppermute | solution.py:44
  352.0 6.5 %collective-permute-done.25 = bf16[128,2048]{1,0:T(8,128)(2,1)S(1)} collective-permute-done((bf16[128,2048]{1,0:T(8,128)(2,1)S(1)}, bf16[128,2048]{1,0:T(8,128)(2,1)S(1)}, u32[]{:S(2)}, u32[]{:S(2)}) %collective-permute-start.25) | collective-permute-done | bytes 524320 | tf_op jit(solution)/shard_map/ppermute | solution.py:44
  360.6 8.8 %stack_landed.5 = (bf16[8,256,1408]{2,1,0:T(8,128)(2,1)}, bf16[8,256,1408]{2,1,0:T(8,128)(2,1)}) custom-call(bf16[2,256,1408]{2,1,0:T(8,128)(2,1)} %collective-permute-done.28.refs_0_, bf16[2,256,1408]{2,1,0:T(8,128)(2,1)} %collective-permute-done.29.refs_1_, bf16[2,256,1408]{2,1,0:T(8,128)(2,1)} %copy-done.6, ...), custom_call_target="tpu_custom_call" | custom-call | tf_op jit(solution)/shard_map/stack_landed/pallas_call | solution.py:102
  369.9 6.5 %fusion.7 = f32[512,1408]{1,0:T(8,128)S(1)} fusion(bf16[2048,1408]{1,0:T(8,128)(2,1)} %bitcast.65, bf16[128,2048]{1,0:T(8,128)(2,1)} %collective-permute-done.47, bf16[128,2048]{1,0:T(8,128)(2,1)S(1)} %collective-permute-done.46, bf16[128,2048]{1,0:T(8,128)(2,1)} %collective-permute-done.45, bf16[128,2048]{1,0:T(8,128)(2,1)S(1)} %multiply_convert_fusion.5), kind=kOutput, calls=%fused_computation.55 | convolution fusion | flops 2961178624 | bytes 10747904 | tf_op jit(solution)/shard_map/dot_general | solution.py:22
  385.5 6.8 %collective-permute-done.26 = bf16[128,2048]{1,0:T(8,128)(2,1)S(1)} collective-permute-done((bf16[128,2048]{1,0:T(8,128)(2,1)S(1)}, bf16[128,2048]{1,0:T(8,128)(2,1)S(1)}, u32[]{:S(2)}, u32[]{:S(2)}) %collective-permute-start.26) | collective-permute-done | bytes 524320 | tf_op jit(solution)/shard_map/ppermute | solution.py:44
  406.1 23.0 %collective-permute-done.40 = bf16[128,2048]{1,0:T(8,128)(2,1)S(1)} collective-permute-done((bf16[128,2048]{1,0:T(8,128)(2,1)S(1)}, bf16[128,2048]{1,0:T(8,128)(2,1)S(1)}, u32[]{:S(2)}, u32[]{:S(2)}) %collective-permute-start.40) | collective-permute-done | bytes 524320 | tf_op jit(solution)/shard_map/ppermute | solution.py:44
  429.3 18.1 %collective-permute-done.48 = bf16[128,2048]{1,0:T(8,128)(2,1)S(1)} collective-permute-done((bf16[128,2048]{1,0:T(8,128)(2,1)S(1)}, bf16[128,2048]{1,0:T(8,128)(2,1)S(1)}, u32[]{:S(2)}, u32[]{:S(2)}) %collective-permute-start.48) | collective-permute-done | bytes 524320 | tf_op jit(solution)/shard_map/ppermute | solution.py:44
  447.4 10.2 %collective-permute-done.39 = bf16[128,2048]{1,0:T(8,128)(2,1)S(1)} collective-permute-done((bf16[128,2048]{1,0:T(8,128)(2,1)S(1)}, bf16[128,2048]{1,0:T(8,128)(2,1)S(1)}, u32[]{:S(2)}, u32[]{:S(2)}) %collective-permute-start.39) | collective-permute-done | bytes 524320 | tf_op jit(solution)/shard_map/ppermute | solution.py:44
  457.6 6.9 %collective-permute-done.41 = bf16[128,2048]{1,0:T(8,128)(2,1)S(1)} collective-permute-done((bf16[128,2048]{1,0:T(8,128)(2,1)S(1)}, bf16[128,2048]{1,0:T(8,128)(2,1)S(1)}, u32[]{:S(2)}, u32[]{:S(2)}) %collective-permute-start.41) | collective-permute-done | bytes 524320 | tf_op jit(solution)/shard_map/ppermute | solution.py:44
  (188 shorter events, 146.6 us)
Async XLA Ops:
  25.8 66.5 %collective-permute-start.27 = (bf16[2,256,1408]{2,1,0:T(8,128)(2,1)S(1)}, bf16[2,256,1408]{2,1,0:T(8,128)(2,1)S(1)}, u32[]{:S(2)}, u32[]{:S(2)}) collective-permute-start(bf16[2,256,1408]{2,1,0:T(8,128)(2,1)S(1)} %pad_maximum_fusion.4), channel_id=1, source_target_pairs={{0,2},{1,3},{2,0},{3,1},{4,6},{5,7},{6,4},{7,5},{8,10},{9,11},{10,... | collective-permute-start | bytes 4325384 | tf_op jit(solution)/shard_map/ppermute | solution.py:44
  40.9 49.6 %collective-permute-start.14 = (bf16[1,256,1408]{2,1,0:T(8,128)(2,1)S(1)}, bf16[1,256,1408]{2,1,0:T(8,128)(2,1)}, u32[]{:S(2)}, u32[]{:S(2)}) collective-permute-start(bf16[1,256,1408]{2,1,0:T(8,128)(2,1)S(1)} %get-tuple-element.33), channel_id=1, source_target_pairs={{0,1},{1,13},{2,3},{3,15},{4,0},{5,4},{6,2},{7,6},{8,9},{9,5},{10,... | collective-permute-start | bytes 2162696 | tf_op jit(solution)/shard_map/ppermute | solution.py:44
  46.4 44.2 %collective-permute-start.2 = (bf16[1,256,1408]{2,1,0:T(8,128)(2,1)}, bf16[1,256,1408]{2,1,0:T(8,128)(2,1)S(1)}, u32[]{:S(2)}, u32[]{:S(2)}) collective-permute-start(bf16[1,256,1408]{2,1,0:T(8,128)(2,1)} %collective-permute-done.1.refs_0_), channel_id=1, source_target_pairs={{0,16},{1,17},{2,18},{3,19},{4,20},{5,21},{6,22},{7,23},{8,24},{9,... | collective-permute-start | bytes 2162696 | tf_op jit(solution)/shard_map/ppermute | solution.py:44
  48.0 46.8 %collective-permute-start.6 = (bf16[1,256,1408]{2,1,0:T(8,128)(2,1)}, bf16[1,256,1408]{2,1,0:T(8,128)(2,1)}, u32[]{:S(2)}, u32[]{:S(2)}) collective-permute-start(bf16[1,256,1408]{2,1,0:T(8,128)(2,1)} %collective-permute-done.5.refs_4_), channel_id=1, source_target_pairs={{0,16},{1,17},{2,18},{3,19},{4,20},{5,21},{6,22},{7,23},{8,24},{9,... | collective-permute-start | bytes 2162696 | tf_op jit(solution)/shard_map/ppermute | solution.py:44
  93.4 33.9 %collective-permute-start.18 = (bf16[1408,512]{1,0:T(8,128)(2,1)}, bf16[1408,512]{1,0:T(8,128)(2,1)}, u32[]{:S(2)}, u32[]{:S(2)}) collective-permute-start(bf16[1408,512]{1,0:T(8,128)(2,1)} %convert_element_type.142.refs_0_), channel_id=1, source_target_pairs={{0,2},{1,3},{2,0},{3,1},{4,6},{5,7},{6,4},{7,5},{8,10},{9,11},{10,... | collective-permute-start | bytes 4325384 | tf_op jit(solution)/shard_map/ppermute | solution.py:44
  104.9 61.2 %collective-permute-start.19 = (bf16[1408,512]{1,0:T(8,128)(2,1)}, bf16[1408,512]{1,0:T(8,128)(2,1)}, u32[]{:S(2)}, u32[]{:S(2)}) collective-permute-start(bf16[1408,512]{1,0:T(8,128)(2,1)} %convert_element_type.142.refs_0_), channel_id=1, source_target_pairs={{0,1},{1,0},{2,3},{3,2},{4,5},{5,4},{6,7},{7,6},{8,9},{9,8},{10,11... | collective-permute-start | bytes 4325384 | tf_op jit(solution)/shard_map/ppermute | solution.py:44
  127.3 38.9 %collective-permute-start.20 = (bf16[1408,512]{1,0:T(8,128)(2,1)}, bf16[1408,512]{1,0:T(8,128)(2,1)}, u32[]{:S(2)}, u32[]{:S(2)}) collective-permute-start(bf16[1408,512]{1,0:T(8,128)(2,1)} %collective-permute-done.18.refs_1_), channel_id=1, source_target_pairs={{0,1},{1,0},{2,3},{3,2},{4,5},{5,4},{6,7},{7,6},{8,9},{9,8},{10,11... | collective-permute-start | bytes 4325384 | tf_op jit(solution)/shard_map/ppermute | solution.py:44
  137.0 104.0 %collective-permute-start.36 = (bf16[1408,512]{1,0:T(8,128)(2,1)S(1)}, bf16[1408,512]{1,0:T(8,128)(2,1)}, u32[]{:S(2)}, u32[]{:S(2)}) collective-permute-start(bf16[1408,512]{1,0:T(8,128)(2,1)S(1)} %copy-done), channel_id=1, source_target_pairs={{0,2},{1,3},{2,0},{3,1},{4,6},{5,7},{6,4},{7,5},{8,10},{9,11},{10,... | collective-permute-start | bytes 4325384 | tf_op jit(solution)/shard_map/ppermute | solution.py:44
  138.0 106.4 %collective-permute-start.28 = (bf16[2,256,1408]{2,1,0:T(8,128)(2,1)}, bf16[2,256,1408]{2,1,0:T(8,128)(2,1)}, u32[]{:S(2)}, u32[]{:S(2)}) collective-permute-start(bf16[2,256,1408]{2,1,0:T(8,128)(2,1)} %get-tuple-element.24), channel_id=1, source_target_pairs={{0,9},{1,5},{2,11},{3,7},{4,8},{5,12},{6,10},{7,14},{8,1},{9,13},{... | collective-permute-start | bytes 4325384 | tf_op jit(solution)/shard_map/ppermute | solution.py:44
  143.1 102.9 %collective-permute-start.32 = (bf16[2,256,1408]{2,1,0:T(8,128)(2,1)}, bf16[2,256,1408]{2,1,0:T(8,128)(2,1)}, u32[]{:S(2)}, u32[]{:S(2)}) collective-permute-start(bf16[2,256,1408]{2,1,0:T(8,128)(2,1)} %get-tuple-element.23), channel_id=1, source_target_pairs={{0,1},{1,13},{2,3},{3,15},{4,0},{5,4},{6,2},{7,6},{8,9},{9,5},{10,... | collective-permute-start | bytes 4325384 | tf_op jit(solution)/shard_map/ppermute | solution.py:44
  227.8 41.0 %collective-permute-start.37 = (bf16[1408,512]{1,0:T(8,128)(2,1)S(1)}, bf16[1408,512]{1,0:T(8,128)(2,1)S(1)}, u32[]{:S(2)}, u32[]{:S(2)}) collective-permute-start(bf16[1408,512]{1,0:T(8,128)(2,1)S(1)} %copy-done), channel_id=1, source_target_pairs={{0,1},{1,0},{2,3},{3,2},{4,5},{5,4},{6,7},{7,6},{8,9},{9,8},{10,11... | collective-permute-start | bytes 4325384 | tf_op jit(solution)/shard_map/ppermute | solution.py:44
  246.0 63.0 %collective-permute-start.33 = (bf16[2,256,1408]{2,1,0:T(8,128)(2,1)}, bf16[2,256,1408]{2,1,0:T(8,128)(2,1)}, u32[]{:S(2)}, u32[]{:S(2)}) collective-permute-start(bf16[2,256,1408]{2,1,0:T(8,128)(2,1)} %collective-permute-done.32.refs_4_), channel_id=1, source_target_pairs={{0,16},{1,17},{2,18},{3,19},{4,20},{5,21},{6,22},{7,23},{8,24},{9,... | collective-permute-start | bytes 4325384 | tf_op jit(solution)/shard_map/ppermute | solution.py:44
  261.2 49.2 %collective-permute-start.38 = (bf16[1408,512]{1,0:T(8,128)(2,1)}, bf16[1408,512]{1,0:T(8,128)(2,1)S(1)}, u32[]{:S(2)}, u32[]{:S(2)}) collective-permute-start(bf16[1408,512]{1,0:T(8,128)(2,1)} %collective-permute-done.36.refs_1_), channel_id=1, source_target_pairs={{0,1},{1,0},{2,3},{3,2},{4,5},{5,4},{6,7},{7,6},{8,9},{9,8},{10,11... | collective-permute-start | bytes 4325384 | tf_op jit(solution)/shard_map/ppermute | solution.py:44
  263.8 47.4 %collective-permute-start.30 = (bf16[2,256,1408]{2,1,0:T(8,128)(2,1)}, bf16[2,256,1408]{2,1,0:T(8,128)(2,1)S(1)}, u32[]{:S(2)}, u32[]{:S(2)}) collective-permute-start(bf16[2,256,1408]{2,1,0:T(8,128)(2,1)} %collective-permute-done.28.refs_0_), channel_id=1, source_target_pairs={{0,1},{1,0},{2,3},{3,2},{4,5},{5,4},{6,7},{7,6},{8,9},{9,8},{10,11... | collective-permute-start | bytes 4325384 | tf_op jit(solution)/shard_map/ppermute | solution.py:44
  268.9 45.2 %collective-permute-start.34 = (bf16[2,256,1408]{2,1,0:T(8,128)(2,1)}, bf16[2,256,1408]{2,1,0:T(8,128)(2,1)S(1)}, u32[]{:S(2)}, u32[]{:S(2)}) collective-permute-start(bf16[2,256,1408]{2,1,0:T(8,128)(2,1)} %collective-permute-done.32.refs_4_), channel_id=1, source_target_pairs={{0,1},{1,0},{2,3},{3,2},{4,5},{5,4},{6,7},{7,6},{8,9},{9,8},{10,11... | collective-permute-start | bytes 4325384 | tf_op jit(solution)/shard_map/ppermute | solution.py:44
  278.1 80.4 %collective-permute-start.31 = (bf16[2,256,1408]{2,1,0:T(8,128)(2,1)}, bf16[2,256,1408]{2,1,0:T(8,128)(2,1)}, u32[]{:S(2)}, u32[]{:S(2)}) collective-permute-start(bf16[2,256,1408]{2,1,0:T(8,128)(2,1)} %collective-permute-done.29.refs_1_), channel_id=1, source_target_pairs={{0,1},{1,0},{2,3},{3,2},{4,5},{5,4},{6,7},{7,6},{8,9},{9,8},{10,11... | collective-permute-start | bytes 4325384 | tf_op jit(solution)/shard_map/ppermute | solution.py:44
  309.0 51.6 %collective-permute-start.35 = (bf16[2,256,1408]{2,1,0:T(8,128)(2,1)}, bf16[2,256,1408]{2,1,0:T(8,128)(2,1)}, u32[]{:S(2)}, u32[]{:S(2)}) collective-permute-start(bf16[2,256,1408]{2,1,0:T(8,128)(2,1)} %collective-permute-done.33.refs_5_), channel_id=1, source_target_pairs={{0,1},{1,0},{2,3},{3,2},{4,5},{5,4},{6,7},{7,6},{8,9},{9,8},{10,11... | collective-permute-start | bytes 4325384 | tf_op jit(solution)/shard_map/ppermute | solution.py:44
  310.5 36.8 %collective-permute-start.46 = (bf16[128,2048]{1,0:T(8,128)(2,1)S(1)}, bf16[128,2048]{1,0:T(8,128)(2,1)S(1)}, u32[]{:S(2)}, u32[]{:S(2)}) collective-permute-start(bf16[128,2048]{1,0:T(8,128)(2,1)S(1)} %multiply_convert_fusion.5), channel_id=1, source_target_pairs={{0,8},{1,9},{2,10},{3,11},{4,12},{5,13},{6,14},{7,15},{8,0},{9,1},... | collective-permute-start | bytes 1572872 | tf_op jit(solution)/shard_map/ppermute | solution.py:44
  311.2 47.4 %collective-permute-start.25 = (bf16[128,2048]{1,0:T(8,128)(2,1)S(1)}, bf16[128,2048]{1,0:T(8,128)(2,1)S(1)}, u32[]{:S(2)}, u32[]{:S(2)}) collective-permute-start(bf16[128,2048]{1,0:T(8,128)(2,1)S(1)} %multiply_convert_fusion.7), channel_id=1, source_target_pairs={{0,8},{1,9},{2,10},{3,11},{4,12},{5,13},{6,14},{7,15},{8,0},{9,1},... | collective-permute-start | bytes 1572872 | tf_op jit(solution)/shard_map/ppermute | solution.py:44
  314.1 55.3 %collective-permute-start.45 = (bf16[128,2048]{1,0:T(8,128)(2,1)S(1)}, bf16[128,2048]{1,0:T(8,128)(2,1)}, u32[]{:S(2)}, u32[]{:S(2)}) collective-permute-start(bf16[128,2048]{1,0:T(8,128)(2,1)S(1)} %multiply_convert_fusion.5), channel_id=1, source_target_pairs={{0,4},{1,5},{2,6},{3,7},{4,0},{5,1},{6,2},{7,3},{8,12},{9,13},{10,... | collective-permute-start | bytes 1572872 | tf_op jit(solution)/shard_map/ppermute | solution.py:44
  403.1 44.3 %collective-permute-start.48 = (bf16[128,2048]{1,0:T(8,128)(2,1)S(1)}, bf16[128,2048]{1,0:T(8,128)(2,1)S(1)}, u32[]{:S(2)}, u32[]{:S(2)}) collective-permute-start(bf16[128,2048]{1,0:T(8,128)(2,1)S(1)} %get-tuple-element.29), channel_id=1, source_target_pairs={{0,4},{1,5},{2,6},{3,7},{4,0},{5,1},{6,2},{7,3},{8,12},{9,13},{10,... | collective-permute-start | bytes 1572872 | tf_op jit(solution)/shard_map/ppermute | solution.py:44
  405.1 52.5 %collective-permute-start.39 = (bf16[128,2048]{1,0:T(8,128)(2,1)S(1)}, bf16[128,2048]{1,0:T(8,128)(2,1)S(1)}, u32[]{:S(2)}, u32[]{:S(2)}) collective-permute-start(bf16[128,2048]{1,0:T(8,128)(2,1)S(1)} %get-tuple-element.25), channel_id=1, source_target_pairs={{0,4},{1,5},{2,6},{3,7},{4,0},{5,1},{6,2},{7,3},{8,12},{9,13},{10,... | collective-permute-start | bytes 1572872 | tf_op jit(solution)/shard_map/ppermute | solution.py:44
  405.3 52.3 %collective-permute-start.50 = (bf16[128,2048]{1,0:T(8,128)(2,1)S(1)}, bf16[128,2048]{1,0:T(8,128)(2,1)S(1)}, u32[]{:S(2)}, u32[]{:S(2)}) collective-permute-start(bf16[128,2048]{1,0:T(8,128)(2,1)S(1)} %add_convert_fusion), channel_id=1, source_target_pairs={{0,8},{1,9},{2,10},{3,11},{4,12},{5,13},{6,14},{7,15},{8,0},{9,1},... | collective-permute-start | bytes 1572872 | tf_op jit(solution)/shard_map/ppermute | solution.py:44
  429.2 35.3 %collective-permute-start.41 = (bf16[128,2048]{1,0:T(8,128)(2,1)S(1)}, bf16[128,2048]{1,0:T(8,128)(2,1)S(1)}, u32[]{:S(2)}, u32[]{:S(2)}) collective-permute-start(bf16[128,2048]{1,0:T(8,128)(2,1)S(1)} %add_convert_fusion.2), channel_id=1, source_target_pairs={{0,8},{1,9},{2,10},{3,11},{4,12},{5,13},{6,14},{7,15},{8,0},{9,1},... | collective-permute-start | bytes 1572872 | tf_op jit(solution)/shard_map/ppermute | solution.py:44
  (52 other events, 1044.3 us)
